TPU v7x, 32 devices: a whole 2x2x4 slice. The times are simulated.
32 devices in a mesh: dp: 4 (over y, x), kv: 4 (over z), tp: 2 (over core).
Axes of the slice: x: 2, y: 2, z: 4, core: 2. Of those that a mesh axis runs over, the one named last changes fastest.
Arguments:
- tokens: bfloat16 [32, 4, 2048], P('dp', None, 'kv'), may hold values from -420 to 420
- input_norm_gain: bfloat16 [2048], replicated, may hold values from 0.099609375 to 1.8984375
- head_input_weight: bfloat16 [2048, 3072], P('kv', 'tp'), may hold values from -0.125 to 0.125
- output_gate_weight: bfloat16 [2048, 3072], P('kv', 'tp'), may hold values from -0.125 to 0.125
- state_maps_weight: bfloat16 [2048, 2, 1024], P('kv', None, 'tp'), may hold values from -0.125 to 0.125
- step_size_weight: bfloat16 [2048, 48], replicated, may hold values from -0.125 to 0.125
- step_size_bias: float32 [48], replicated, may hold values from -4 to -1
- head_decay_speed: float32 [48], replicated, may hold values from 0.3 to 8
- proposal_decay_total: float32 [32, 4, 48], P(('dp', 'kv'), None, 'tp'), may hold values from -0.7 to 0
- head_input_kernel: bfloat16 [4, 3072], replicated, may hold values from -3 to 3
- state_maps_kernel: bfloat16 [4, 2, 1024], replicated, may hold values from -3 to 3
- head_direct_gain: float32 [48], replicated, may hold values from 0.5 to 1.5
- grouped_norm_gain: bfloat16 [3072], replicated, may hold values from 0.099609375 to 1.8984375
- output_weight: bfloat16 [3072, 2048], P('tp', 'kv'), may hold values from -0.109375 to 0.109375
- prior_state_value: float32 [32, 48, 64, 128], P(('dp', 'kv'), 'tp'), may hold values from -2.4 to 2.4
- previous_head_input: bfloat16 [32, 4, 3072], P(('dp', 'kv'), None, 'tp'), may hold values from -2.390625 to 2.390625
- previous_input_maps: bfloat16 [32, 4, 1024], P(('dp', 'kv'), None, 'tp'), may hold values from -5 to 5
- previous_log_decays: float32 [32, 4, 48], P(('dp', 'kv'), None, 'tp'), may hold values from -1.5 to -0.05
- prior_heads_window: bfloat16 [32, 7, 3072], P(('dp', 'kv'), None, 'tp'), may hold values from -6 to 6
- prior_maps_window: bfloat16 [32, 7, 2, 1024], P(('dp', 'kv'), None, None, 'tp'), may hold values from -6 to 6
- accepted: int32 [32], P(('dp', 'kv')), may hold values from 1 to 4
Outputs:
- mixed: bfloat16 [32, 4, 2048], P('dp', None, 'kv')
- accepted_state: float32 [32, 48, 64, 128], P(('dp', 'kv'), 'tp')
- current_head_input: bfloat16 [32, 4, 3072], P(('dp', 'kv'), None, 'tp')
- current_input_maps: bfloat16 [32, 4, 1024], P(('dp', 'kv'), None, 'tp')
- current_log_decays: float32 [32, 4, 48], P(('dp', 'kv'), None, 'tp')
- current_heads_window: bfloat16 [32, 7, 3072], P(('dp', 'kv'), None, 'tp')
- current_maps_window: bfloat16 [32, 7, 2, 1024], P(('dp', 'kv'), None, None, 'tp')
All inputs are finite; a program needn't handle non-finite values.
Results may differ from a plain program's by a relative error of at most 0.029.
Values may be sent and summed in bfloat16 or wider, within the bound.
No kernel may reach another device: no remote copies, remote signals or barrier semaphores. Data moves between devices by JAX's collectives and lax.ppermute only.
A program may use at most 64 MiB of HBM per device.

v0:
```python
import jax
import jax.numpy as jnp
from jax import lax
from jax.sharding import PartitionSpec as P

D = 2048
HEAD_DIM = 64
STATE = 128
CONV = 4


eps = 1e-06


def shortened(array):

    def short(part):
        return part.astype(jnp.bfloat16) if part.dtype == jnp.float32 else part

    return jax.tree.map(short, array)


def pick_tail(history, accepted):
    rows = history.shape[1]
    keep = CONV - 1
    index = jnp.arange(rows, dtype=jnp.int32)
    offsets = jnp.arange(keep, dtype=jnp.int32)
    select = (index[None, None, :] == accepted[:, None, None] + offsets[None, :, None]).astype(
        jnp.float32
    )
    flat = history.astype(jnp.float32).reshape(history.shape[0], rows, -1)
    picked = jnp.einsum("skr,src->skc", select, flat, precision=lax.Precision.HIGHEST)
    return picked.reshape((history.shape[0], keep) + history.shape[2:])


def causal_conv(window, weight):
    length = window.shape[1] - CONV + 1
    total = weight[0] * window[:, 0:length]
    for offset in range(1, CONV):
        total = total + weight[offset] * window[:, offset : offset + length]
    return jax.nn.silu(total)


def local_mixer_output(
    unfiltered_heads,
    gate_logits,
    unfiltered_maps,
    step_logits,
    prior_heads_window,
    prior_maps_window,
    accepted,
    proposal_run,
    prior_state_value,
    previous_head_input,
    previous_input_maps,
    previous_log_decays,
    head_input_kernel,
    state_maps_kernel,
    step_size_bias,
    head_decay_speed,
    head_direct_gain,
    grouped_norm_gain,
):
    seqs, props, width = unfiltered_heads.shape
    heads = step_logits.shape[2]
    groups = unfiltered_maps.shape[3] // STATE
    repeat = heads // groups
    tail_x = pick_tail(prior_heads_window, accepted)
    tail_bc = pick_tail(prior_maps_window, accepted)
    window_x = jnp.concatenate([tail_x, unfiltered_heads.astype(jnp.float32)], axis=1)
    window_bc = jnp.concatenate([tail_bc, unfiltered_maps.astype(jnp.float32)], axis=1)
    current_heads_window = window_x.astype(jnp.bfloat16)
    current_maps_window = window_bc.astype(jnp.bfloat16)
    x_conv = causal_conv(window_x, head_input_kernel.astype(jnp.float32)).reshape(
        seqs, props, heads, HEAD_DIM
    )
    bc_conv = causal_conv(window_bc, state_maps_kernel.astype(jnp.float32)).reshape(
        seqs, props, 2, groups, STATE
    )
    b_conv = bc_conv[:, :, 0]
    c_conv = bc_conv[:, :, 1]
    positive_step_size = jax.nn.softplus(step_logits + step_size_bias)
    logarithm_decay = proposal_run - head_decay_speed * positive_step_size
    weighted = positive_step_size[..., None] * x_conv
    current_head_input = weighted.reshape(seqs, props, width).astype(jnp.bfloat16)
    current_input_maps = b_conv.reshape(seqs, props, groups * STATE).astype(jnp.bfloat16)
    past_heads = previous_head_input.astype(jnp.float32).reshape(seqs, props, heads, HEAD_DIM)
    past_keys = jnp.repeat(
        previous_input_maps.astype(jnp.float32).reshape(seqs, props, groups, STATE), repeat, axis=2
    )
    carried = prior_state_value
    for position in range(props):
        keep = (position < accepted).astype(jnp.float32)[:, None]
        factor = jnp.exp(keep * previous_log_decays[:, position])
        update = past_heads[:, position, :, :, None] * past_keys[:, position, :, None, :]
        carried = carried * factor[:, :, None, None] + keep[:, :, None, None] * update
    cumulative = jnp.cumsum(logarithm_decay, axis=1)
    c_heads = jnp.repeat(c_conv, repeat, axis=2)
    b_heads = jnp.repeat(b_conv, repeat, axis=2)
    from_state = jnp.exp(cumulative)[..., None] * jnp.einsum(
        "sthn,shpn->sthp", c_heads, carried, precision=lax.Precision.HIGHEST
    )
    order = jnp.arange(props)
    causal = (order[:, None] >= order[None, :])[None, :, :, None]
    spread_log = cumulative[:, :, None, :] - cumulative[:, None, :, :]
    decay = jnp.where(causal, jnp.exp(jnp.where(causal, spread_log, 0.0)), 0.0)
    scores = (
        jnp.einsum("sthn,suhn->stuh", c_heads, b_heads, precision=lax.Precision.HIGHEST) * decay
    )
    within = jnp.einsum("stuh,suhp->sthp", scores, weighted, precision=lax.Precision.HIGHEST)
    heads_out = from_state + within + head_direct_gain[:, None] * x_conv
    gated = heads_out.reshape(seqs, props, width) * jax.nn.silu(gate_logits)
    grouped = gated.reshape(seqs, props, groups, width // groups)
    grouped = grouped * lax.rsqrt(jnp.mean(grouped * grouped, axis=-1, keepdims=True) + eps)
    normalized_input = (
        grouped.reshape(seqs, props, width) * grouped_norm_gain.astype(jnp.float32)
    ).astype(jnp.bfloat16)
    return (
        normalized_input,
        carried,
        current_head_input,
        current_input_maps,
        logarithm_decay,
        current_heads_window,
        current_maps_window,
    )


def local(
    tokens,
    input_norm_gain,
    head_input_weight,
    output_gate_weight,
    state_maps_weight,
    step_size_weight,
    step_size_bias,
    head_decay_speed,
    proposal_decay_total,
    head_input_kernel,
    state_maps_kernel,
    head_direct_gain,
    grouped_norm_gain,
    output_weight,
    prior_state_value,
    previous_head_input,
    previous_input_maps,
    previous_log_decays,
    prior_heads_window,
    prior_maps_window,
    accepted,
):
    kv_index = lax.axis_index("kv")
    tp_index = lax.axis_index("tp")
    seq_rows, props, local_d = tokens.shape
    local_heads = step_size_weight.shape[1] // lax.axis_size("tp")
    local_width = head_input_weight.shape[1]
    local_bc = state_maps_weight.shape[2]
    own_seqs = prior_state_value.shape[0]
    own_rows = own_seqs * props
    own_start = kv_index * own_rows
    head_start = tp_index * local_heads
    values = tokens.astype(jnp.float32)
    sumsq = jnp.sum(values * values, axis=-1).reshape(seq_rows * props)
    row_total = lax.psum(sumsq, "kv")
    own_sumsq = lax.dynamic_slice_in_dim(row_total, own_start, own_rows, 0)
    gain_part = lax.dynamic_slice_in_dim(input_norm_gain, kv_index * local_d, local_d, 0)
    scaled = (
        (values * gain_part.astype(jnp.float32))
        .astype(jnp.bfloat16)
        .reshape(seq_rows * props, local_d)
    )
    step_part = lax.dynamic_slice(
        step_size_weight, (kv_index * local_d, head_start), (local_d, local_heads)
    )
    proj_x = jnp.dot(scaled, head_input_weight, preferred_element_type=jnp.float32)
    proj_gate = jnp.dot(scaled, output_gate_weight, preferred_element_type=jnp.float32)
    proj_bc = jnp.dot(
        scaled, state_maps_weight.reshape(local_d, 2 * local_bc), preferred_element_type=jnp.float32
    )
    proj_step = jnp.dot(scaled, step_part, preferred_element_type=jnp.float32)
    members = (proj_x, proj_gate, proj_bc, proj_step) + ()
    summed = jax.tree.map(lambda part: part.astype(jnp.float32), lax.psum(shortened(members), "kv"))
    summed = tuple((lax.dynamic_slice_in_dim(member, own_start, own_rows, 0) for member in summed))
    inv_rms = lax.rsqrt(own_sumsq / D + eps)[:, None]
    unfiltered_heads = (
        (summed[0] * inv_rms).astype(jnp.bfloat16).reshape(own_seqs, props, local_width)
    )
    gate_logits = (summed[1] * inv_rms).reshape(own_seqs, props, local_width)
    unfiltered_maps = (
        (summed[2] * inv_rms).astype(jnp.bfloat16).reshape(own_seqs, props, 2, local_bc)
    )
    step_logits = (summed[3] * inv_rms).reshape(own_seqs, props, local_heads)
    bias_part = lax.dynamic_slice_in_dim(step_size_bias, head_start, local_heads, 0)
    rate_part = lax.dynamic_slice_in_dim(head_decay_speed, head_start, local_heads, 0)
    skip_part = lax.dynamic_slice_in_dim(head_direct_gain, head_start, local_heads, 0)
    conv_x_part = lax.dynamic_slice_in_dim(
        head_input_kernel, tp_index * local_width, local_width, 1
    )
    conv_bc_part = lax.dynamic_slice_in_dim(state_maps_kernel, tp_index * local_bc, local_bc, 2)
    out_gain_part = lax.dynamic_slice_in_dim(
        grouped_norm_gain, tp_index * local_width, local_width, 0
    )
    (
        normalized_input,
        accepted_state,
        current_head_input,
        current_input_maps,
        current_log_decays,
        current_heads_window,
        current_maps_window,
    ) = local_mixer_output(
        unfiltered_heads,
        gate_logits,
        unfiltered_maps,
        step_logits,
        prior_heads_window,
        prior_maps_window,
        accepted,
        proposal_decay_total,
        prior_state_value,
        previous_head_input,
        previous_input_maps,
        previous_log_decays,
        conv_x_part,
        conv_bc_part,
        bias_part,
        rate_part,
        skip_part,
        out_gain_part,
    )
    flat = normalized_input.reshape(own_rows, local_width)
    partial_value = jnp.dot(
        lax.all_gather(flat, "kv", axis=0, tiled=True),
        output_weight,
        preferred_element_type=jnp.float32,
    )
    mixed = lax.psum(partial_value.astype(jnp.bfloat16), "tp")
    return (
        mixed.reshape(seq_rows, props, local_d),
        accepted_state,
        current_head_input,
        current_input_maps,
        current_log_decays,
        current_heads_window,
        current_maps_window,
    )


def solution(mesh):
    return jax.shard_map(
        local,
        mesh=mesh,
        in_specs=(
            P("dp", None, "kv"),
            P(),
            P("kv", "tp"),
            P("kv", "tp"),
            P("kv", None, "tp"),
            P(),
            P(),
            P(),
            P(("dp", "kv"), None, "tp"),
            P(),
            P(),
            P(),
            P(),
            P("tp", "kv"),
            P(("dp", "kv"), "tp", None, None),
            P(("dp", "kv"), None, "tp"),
            P(("dp", "kv"), None, "tp"),
            P(("dp", "kv"), None, "tp"),
            P(("dp", "kv"), None, "tp"),
            P(("dp", "kv"), None, None, "tp"),
            P(("dp", "kv")),
        ),
        out_specs=(
            P("dp", None, "kv"),
            P(("dp", "kv"), "tp", None, None),
            P(("dp", "kv"), None, "tp"),
            P(("dp", "kv"), None, "tp"),
            P(("dp", "kv"), None, "tp"),
            P(("dp", "kv"), None, "tp"),
            P(("dp", "kv"), None, None, "tp"),
        ),
        check_vma=False,
    )
```

profile of v0, /device:TPU:0, one launch (start us, length us, event | category | flops | bytes accessed | tf_op | source)
XLA Modules:
  0.0 88.5 jit_solution(11254030108223856802)
XLA Ops:
  7.2 0.9 %dynamic-slice_convert_fusion.3 = f32[512]{0:T(512)S(1)} fusion(bf16[2048]{0:T(1024)(128)(2,1)} %param.22, s32[]{:T(128)S(6)} %select_n.40), kind=kLoop, calls=%fused_computation.93 | loop fusion | flops 512 | bytes 3076 | tf_op jit(solution)/shard_map/convert_element_type | solution.py:168
  8.2 0.9 fusion.6
  9.1 1.0 %convolution_convert_fusion = bf16[32,1536]{1,0:T(8,128)(2,1)} fusion(bf16[32,512]{1,0:T(8,128)(2,1)S(1)} %reshape.263, bf16[512,1536]{1,0:T(8,128)(2,1)S(1)} %copy-done), kind=kOutput, calls=%fused_computation | convolution fusion | flops 50380800 | bytes 1703936 | tf_op jit(solution)/shard_map/dot_general | solution.py:176
  10.1 1.0 %convolution_convert_fusion.1 = bf16[32,1536]{1,0:T(8,128)(2,1)} fusion(bf16[32,512]{1,0:T(8,128)(2,1)S(1)} %reshape.263, bf16[512,1536]{1,0:T(8,128)(2,1)S(1)} %copy-done.2), kind=kOutput, calls=%fused_computation.1 | convolution fusion | flops 50380800 | bytes 1703936 | tf_op jit(solution)/shard_map/dot_general | solution.py:175
  11.2 0.2 copy.138
  11.5 0.9 %convolution_convert_fusion.2 = bf16[32,1024]{1,0:T(8,128)(2,1)} fusion(bf16[32,512]{1,0:T(8,128)(2,1)S(1)} %reshape.263, bf16[512,1024]{1,0:T(8,128)(2,1)S(1)} %bitcast.81), kind=kOutput, calls=%fused_computation.5 | convolution fusion | flops 33587200 | bytes 1146880 | tf_op jit(solution)/shard_map/dot_general | solution.py:177
  12.5 0.1 dynamic_slice.44
  12.6 0.1 dynamic_slice.39
  12.7 0.7 dynamic-slice_convert_fusion.2
  13.4 0.7 slice_reduce_fusion.3
  14.1 0.2 fusion.24
  14.3 0.1 reshape.264
  14.4 13.6 %psum.43 = f32[32]{0:T(128)S(1)} all-reduce(f32[32]{0:T(128)S(1)} %reshape.264), channel_id=1, replica_groups=mesh['dp'=4,'kv'=4,'tp'=2] {'kv'}, use_global_device_ids=true, to_apply=%region_2.0 | all-reduce | flops 32 | bytes 256 | tf_op jit(solution)/shard_map/psum | solution.py:164
  28.0 0.9 convolution_convert_fusion.4
  28.8 8.5 %psum.42 = bf16[32,24]{1,0:T(8,128)(2,1)S(1)} all-reduce(bf16[32,24]{1,0:T(8,128)(2,1)S(1)} %convolution_convert_fusion.4), channel_id=1, replica_groups=mesh['dp'=4,'kv'=4,'tp'=2] {'kv'}, use_global_device_ids=true, to_apply=%region_0.0 | all-reduce | flops 768 | bytes 3072 | tf_op jit(solution)/shard_map/psum | solution.py:182
  37.5 0.1 reshape.282
  37.6 0.1 add_rsqrt_fusion.1
  37.7 0.1 multiply_exponential_fusion.2
  37.8 0.1 multiply_exponential_fusion
  38.0 4.0 %multiply_add_fusion = f32[2,24,64,128]{3,2,1,0:T(8,128)S(1)} fusion(f32[2,24,64,128]{3,2,1,0:T(8,128)} %param.35, f32[2,24,128]{2,1,0:T(8,128)S(1)} %bitcast.89, f32[2,24,64]{2,1,0:T(8,128)S(1)} %get-tuple-element.58, f32[2]{0:T(128)S(1)} %get-tuple-element.78, f32[2,24]{1,0:T(2,128)S(1)} %get-tuple-element.81, f32[2,24,128]{2,1,0:T(8,128)S(1)} %bitcast.90, ...), kind=kLoop, calls=%fused_computation.2 | loop fusion | flops 6291456 | bytes 3293984 | tf_op jit(solution)/shard_map/add | solution.py:96
  42.0 0.6 iota_compare_fusion.3
  42.6 0.7 copy.122
  43.3 0.6 dynamic_slice.49
  43.9 0.1 mul.481
  44.0 0.1 mul.513
  44.1 0.2 fusion.16
  44.3 6.9 %all-reduce.3.cloned.1.call-done = (bf16[32,1024]{1,0:T(8,128)(2,1)}, bf16[32,1536]{1,0:T(8,128)(2,1)}, bf16[32,1536]{1,0:T(8,128)(2,1)}) async-done(((bf16[32,1024]{1,0:T(8,128)(2,1)}, bf16[32,1536]{1,0:T(8,128)(2,1)}, bf16[32,1536]{1,0:T(8,128)(2,1)}), (bf16[32,1024]{1,0:T(8,128)(2,1)}, bf16[32,1536]{1,0:T(8,128)(2,1)}, bf16[32,1536]{1,0:T(8,128)(2,1)})) %all-reduce.3.cloned.1.call-update) | async-done | bytes 262160 | tf_op jit(solution)/shard_map/psum | solution.py:182
  51.2 0.8 fusion.23
  52.0 0.6 convert_element_type.130
  52.8 0.6 convert_element_type.128
  53.4 0.8 fusion.21
  54.3 0.7 copy.129
  55.0 1.4 %multiply_convert_fusion = (bf16[2,4,1536]{2,1,0:T(4,128)(2,1)}, f32[2,4,1536]{2,1,0:T(4,128)S(1)}) fusion(f32[2,4,1536]{2,1,0:T(4,128)S(1)} %mul.513, f32[2,4,1536]{2,1,0:T(4,128)S(1)} %reshape.286, f32[1536]{0:T(1024)S(1)} %get-tuple-element.43, f32[1536]{0:T(1024)S(1)} %get-tuple-element.44, f32[1536]{0:T(1024)} %get-tuple-element.45, ...), kind=kLoop, calls=%fused_computation.38 | loop fusion | flops 196608 | bytes 233472 | tf_op jit(solution)/shard_map/convert_element_type | solution.py:85
  56.4 0.1 reshape.276
  56.5 0.1 broadcast_multiply_fusion
  56.6 0.1 reshape.279
  56.7 2.5 %fusion.30 = f32[2,24,64,4]{2,3,1,0:T(4,128)S(1)} fusion(f32[2,24,64,128]{3,2,1,0:T(8,128)S(1)} %multiply_add_fusion, f32[2,4,24,128]{3,1,2,0:T(4,128)S(1)} %bitcast.83), kind=kOutput, calls=%fused_computation.97 | convolution fusion | flops 18874368 | bytes 1720320 | tf_op jit(solution)/shard_map/sthn,shpn->sthp/dot_general | solution.py:100
  59.3 1.3 %fusion = f32[2,4,4,24]{1,2,3,0:T(4,128)S(1)} fusion(f32[2,4,24,128]{3,1,2,0:T(4,128)S(1)} %bitcast.92, f32[2,4,24,128]{3,1,2,0:T(4,128)S(1)} %bitcast.84, f32[2,4,24]{1,2,0:T(8,128)} %copy.122, pred[4,4]{0,1:T(4,128)(4,1)} %iota_compare_fusion.3), kind=kOutput, calls=%fused_computation.4 | convolution fusion | flops 1182720 | bytes 200464 | tf_op jit(solution)/shard_map/sthn,suhn->stuh/dot_general | solution.py:108
  60.6 0.6 fusion.3
  61.1 0.2 multiply_reduce_fusion
  61.3 0.1 reduce_sum.27
  61.4 0.1 reduce_sum.28
  61.5 0.1 mul.508
  61.6 0.1 reshape.278
  61.7 0.8 multiply_convert_fusion.1
  62.6 13.3 %all_gather.3 = bf16[32,1536]{1,0:T(8,128)(2,1)S(1)} all-gather(bf16[8,1536]{1,0:T(8,128)(2,1)S(1)} %multiply_convert_fusion.1), channel_id=1, replica_groups=mesh['dp'=4,'kv'=4,'tp'=2] {'kv'}, dimensions={0}, use_global_device_ids=true | all-gather | bytes 122880 | tf_op jit(solution)/shard_map/all_gather | solution.py:233
  75.9 1.8 %convolution_convert_fusion.3 = bf16[32,512]{1,0:T(8,128)(2,1)S(1)} fusion(bf16[32,1536]{1,0:T(8,128)(2,1)S(1)} %all_gather.3, bf16[1536,512]{1,0:T(8,128)(2,1)} %param.34), kind=kOutput, calls=%fused_computation.6 | convolution fusion | flops 50348032 | bytes 1703936 | tf_op jit(solution)/shard_map/dot_general | solution.py:232
  77.7 4.0 %psum.47 = bf16[8,4,512]{2,1,0:T(4,128)(2,1)} all-reduce(bf16[8,4,512]{2,1,0:T(4,128)(2,1)S(1)} %reshape.280), channel_id=1, replica_groups=mesh['dp'=4,'kv'=4,'tp'=2] {'tp'}, use_global_device_ids=true, to_apply=%region_9.10 | all-reduce | flops 16384 | bytes 65536 | tf_op jit(solution)/shard_map/psum | solution.py:237
  (79 shorter events, 0.9 us)
Async XLA Ops:
  7.2 1.9 %copy-start = (bf16[512,1536]{1,0:T(8,128)(2,1)S(1)}, bf16[512,1536]{1,0:T(8,128)(2,1)}, u32[]{:S(2)}) copy-start(bf16[512,1536]{1,0:T(8,128)(2,1)} %param.24) | copy-start | bytes 4718596
  7.2 2.9 %copy-start.2 = (bf16[512,1536]{1,0:T(8,128)(2,1)S(1)}, bf16[512,1536]{1,0:T(8,128)(2,1)}, u32[]{:S(2)}) copy-start(bf16[512,1536]{1,0:T(8,128)(2,1)} %param.23) | copy-start | bytes 4718596
  7.2 44.0 %all-reduce.3.cloned.1.call-start = ((), (), s32[]{:S(2)}) async-start(), calls=%async_computation | async-start | bytes 524288 | tf_op jit(solution)/shard_map/psum | solution.py:182
  9.0 2.1 %copy-start.3 = (bf16[512,2,512]{2,1,0:T(2,128)(2,1)S(1)}, bf16[512,2,512]{2,1,0:T(2,128)(2,1)}, u32[]{:S(2)}) copy-start(bf16[512,2,512]{2,1,0:T(2,128)(2,1)} %param.25) | copy-start | bytes 3145732
  11.1 1.3 %copy-start.18 = (s32[2]{0:T(128)S(1)}, s32[2]{0:T(128)}, u32[]{:S(2)}) copy-start(s32[2]{0:T(128)} %param.41) | copy-start | bytes 28
  11.1 1.4 %copy-start.19 = (f32[48]{0:T(128)S(1)}, f32[48]{0:T(128)}, u32[]{:S(2)}) copy-start(f32[48]{0:T(128)} %param.27) | copy-start | bytes 580
  11.1 1.5 %copy-start.20 = (f32[48]{0:T(128)S(1)}, f32[48]{0:T(128)}, u32[]{:S(2)}) copy-start(f32[48]{0:T(128)} %param.28) | copy-start | bytes 580
  11.1 1.5 %copy-start.15 = (f32[2,4,24]{2,1,0:T(4,128)S(1)}, f32[2,4,24]{2,1,0:T(4,128)}, u32[]{:S(2)}) copy-start(f32[2,4,24]{2,1,0:T(4,128)} %param.38) | copy-start | bytes 2308
  11.1 1.5 %copy-start.13 = (bf16[4,2,1024]{2,1,0:T(2,128)(2,1)S(1)}, bf16[4,2,1024]{2,1,0:T(2,128)(2,1)}, u32[]{:S(2)}) copy-start(bf16[4,2,1024]{2,1,0:T(2,128)(2,1)} %param.31) | copy-start | bytes 49156
  11.1 1.6 %copy-start.11 = (bf16[2,4,512]{2,1,0:T(4,128)(2,1)S(1)}, bf16[2,4,512]{2,1,0:T(4,128)(2,1)}, u32[]{:S(2)}) copy-start(bf16[2,4,512]{2,1,0:T(4,128)(2,1)} %param.37) | copy-start | bytes 24580
  11.1 1.6 %copy-start.16 = (bf16[3072]{0:T(1024)(128)(2,1)S(1)}, bf16[3072]{0:T(1024)(128)(2,1)}, u32[]{:S(2)}) copy-start(bf16[3072]{0:T(1024)(128)(2,1)} %param.33) | copy-start | bytes 18436
  11.2 2.2 %copy-start.12 = (bf16[4,3072]{1,0:T(4,128)(2,1)S(1)}, bf16[4,3072]{1,0:T(4,128)(2,1)}, u32[]{:S(2)}) copy-start(bf16[4,3072]{1,0:T(4,128)(2,1)} %param.30) | copy-start | bytes 73732
  11.2 2.9 %copy-start.6 = (bf16[2,7,2,512]{3,2,1,0:T(2,128)(2,1)S(1)}, bf16[2,7,2,512]{3,2,1,0:T(2,128)(2,1)}, u32[]{:S(2)}) copy-start(bf16[2,7,2,512]{3,2,1,0:T(2,128)(2,1)} %param.40) | copy-start | bytes 86020
  11.4 26.0 %copy-start.7 = (bf16[2,4,1536]{2,1,0:T(4,128)(2,1)S(1)}, bf16[2,4,1536]{2,1,0:T(4,128)(2,1)}, u32[]{:S(2)}) copy-start(bf16[2,4,1536]{2,1,0:T(4,128)(2,1)} %param.36) | copy-start | bytes 73732
  11.4 26.5 %copy-start.14 = (f32[2,4,24]{2,1,0:T(4,128)S(1)}, f32[2,4,24]{2,1,0:T(4,128)}, u32[]{:S(2)}) copy-start(f32[2,4,24]{2,1,0:T(4,128)} %param.29) | copy-start | bytes 2308
  37.7 13.5 %copy-start.9 = (f32[8]{0:T(128)}, f32[8]{0:T(128)S(1)}, u32[]{:S(2)}) copy-start(f32[8]{0:T(128)S(1)} %add_rsqrt_fusion.1) | copy-start | bytes 100
  37.9 4.6 %copy-start.8 = (f32[2,4,24]{2,1,0:T(4,128)}, f32[2,4,24]{2,1,0:T(4,128)S(1)}, u32[]{:S(2)}) copy-start(f32[2,4,24]{2,1,0:T(4,128)S(1)} %get-tuple-element.53) | copy-start | bytes 2308
  37.9 5.3 %copy-start.21 = (f32[48]{0:T(128)S(1)}, f32[48]{0:T(128)}, u32[]{:S(2)}) copy-start(f32[48]{0:T(128)} %param.32) | copy-start | bytes 580
  38.0 6.2 %copy-start.4 = (bf16[2,7,1536]{2,0,1:T(2,128)(2,1)S(1)}, bf16[2,7,1536]{2,0,1:T(2,128)(2,1)}, u32[]{:S(2)}) copy-start(bf16[2,7,1536]{2,0,1:T(2,128)(2,1)} %param.39) | copy-start | bytes 129028
  42.0 17.3 %copy-start.1 = (f32[2,24,64,128]{3,2,1,0:T(8,128)}, f32[2,24,64,128]{3,2,1,0:T(8,128)S(1)}, u32[]{:S(2)}) copy-start(f32[2,24,64,128]{3,2,1,0:T(8,128)S(1)} %multiply_add_fusion) | copy-start | bytes 4718596
  56.5 4.6 %copy-start.17 = (f32[24]{0:T(128)S(1)}, f32[24]{0:T(128)}, u32[]{:S(2)}) copy-start(f32[24]{0:T(128)} %dynamic_slice.49) | copy-start | bytes 292
  56.7 5.0 %copy-start.5 = (f32[1536]{0:T(1024)S(1)}, f32[1536]{0:T(1024)}, u32[]{:S(2)}) copy-start(f32[1536]{0:T(1024)} %dynamic-slice_convert_fusion.2) | copy-start | bytes 18436
  56.7 5.0 %copy-start.10 = (f32[8]{0:T(128)S(1)}, f32[8]{0:T(128)}, u32[]{:S(2)}) copy-start(f32[8]{0:T(128)} %copy-done.9) | copy-start | bytes 100
Sparse Core Ops, SparseCore 0:
  12.5 38.6 all-reduce.2
where the time goes:
time: 89.1 us; the launch traced here: 88.5 us
  blocking collectives  39.4 us (44%)
  between operations  14.5 us (16%)
  other arithmetic  12.5 us (14%)
  matrix products  10.3 us (12%)
  waiting for transfers between devices  6.89 us (8%)
  local copies, waits for them, and re-layouts  4.94 us (6%)
    psum x1, blocking collectives, local(): row_total = lax.psum(sumsq, 'kv')  13.6 us
    all_gather x1, blocking collectives, local(): lax.all_gather(flat, 'kv', axis=0, tiled=True)  13.3 us
    psum x1, blocking collectives, local(): lax.psum(shortened(members), 'kv')  8.52 us
    psum x1, waiting for transfers between devices, local(): lax.psum(shortened(members), 'kv')  6.87 us
    psum x1, blocking collectives, local(): mixed = lax.psum(partial_value.astype(jnp.bfloat16), 'tp')  4 us
    add x1, other arithmetic, local_mixer_output(): carried * factor[:, :, None, None] + keep[:, :, None, None] * update  3.97 us
    dot_general x1, matrix products, local_mixer_output(): jnp.einsum('sthn,shpn->sthp', c_heads, carried, precision=lax.Precision.H...  2.54 us
  transfers between devices with their start and end apart: 1, of which 1 were waited for; matrix products, arithmetic and copies ran while one was open for 11% of the time, Pallas kernels for 0%

commit v1 on v0

v1 whole, which is shorter than its diff:
```python
import functools

import jax
import jax.numpy as jnp
from jax import lax
from jax.experimental import pallas as pl
from jax.experimental.pallas import tpu as pltpu
from jax.sharding import PartitionSpec as P

HEAD_DIM = 64
STATE = 128
CONV = 4
LANES = 128
DIRECT = 8

eps = 1e-06
f32 = jnp.float32
bf16 = jnp.bfloat16

NT = (((1,), (1,)), ((), ()))
TN = (((0,), (0,)), ((), ()))


def params(mib):
    return pltpu.CompilerParams(vmem_limit_bytes=mib << 20)


def peer(me, k, n, back=False):
    if n > DIRECT:
        return k
    if n & (n - 1) == 0:
        return me ^ k
    return lax.rem(me + (n - k if back else k), n)


def permute(array, axis, k, n):
    return lax.ppermute(array, axis, [(i, int(peer(i, k, n))) for i in range(n)])


def pick(rows, index, count, width):
    out = rows[:, :width]
    for block in range(1, count):
        out = jnp.where(index == block, rows[:, block * width : (block + 1) * width], out)
    return out


def spread(values, heads):
    rows = values.shape[0]
    per = LANES // HEAD_DIM
    lane = lax.broadcasted_iota(jnp.int32, (rows, LANES), 1)
    tiles = []
    for first in range(0, heads, per):
        tile = jnp.broadcast_to(values[:, first : first + 1], (rows, LANES))
        for j in range(1, per):
            other = jnp.broadcast_to(values[:, first + j : first + j + 1], (rows, LANES))
            tile = jnp.where(lane >= j * HEAD_DIM, other, tile)
        tiles.append(tile)
    return jnp.concatenate(tiles, axis=1)


def silu(x):
    return x * (1.0 / (1.0 + jnp.exp(-x)))


def project_kernel(n_kv, n_heads, tok, gain, wx, wm, wg, ws, *outs):
    kv = lax.axis_index("kv")
    seqs, props, local_d = tok.shape
    own = seqs // n_kv
    rows = own * props
    parts, squares = [], []
    for k in range(n_kv):
        start = peer(kv, k, n_kv) * own
        for s in range(own):
            values = tok[start + s].astype(f32)
            parts.append(values)
    values = jnp.concatenate(parts, axis=0)
    squares = jnp.sum(values * values, axis=1, keepdims=True)
    scaled = (values * gain[...]).astype(bf16)
    high = squares.astype(bf16).astype(f32)
    step = lax.dot_general(scaled, ws[...], NT, preferred_element_type=f32)
    lane = lax.broadcasted_iota(jnp.int32, step.shape, 1)
    step = jnp.where(lane == n_heads, high, jnp.where(lane == n_heads + 1, squares - high, step))
    at = 0
    for block in (wx, wm, wg):
        width = block.shape[1]
        part = jnp.dot(scaled, block[...], preferred_element_type=f32)
        for k in range(n_kv):
            outs[k][:, at : at + width] = part[k * rows : (k + 1) * rows].astype(bf16)
        at += width
    for k in range(n_kv):
        outs[k][:, at:] = step[k * rows : (k + 1) * rows].astype(bf16)


def state_kernel(
    n_tp,
    acc,
    state,
    past_x,
    past_maps,
    past_logs,
    heads_window,
    maps_window,
    head_taps,
    map_taps,
    bias,
    speed,
    direct,
    norm_gain,
    new_state,
    state_low,
    tail_x,
    tail_maps,
    conv_tail,
    taps,
    vectors,
    small,
    gain_rows,
):
    tp = lax.axis_index("tp")
    own, heads = state.shape[:2]
    props, width = past_x.shape[1:]
    bc = past_maps.shape[2]
    groups = bc // STATE
    per_group = heads // groups
    group_width = per_group * HEAD_DIM
    keep = CONV - 1

    head_cols = pl.ds(pl.multiple_of(tp * width, LANES), width)
    map_cols = pl.ds(pl.multiple_of(tp * bc, LANES), bc)
    weight_x = head_taps[:, head_cols].astype(f32)
    taps[:, :width] = weight_x
    weight_b, weight_c = [], []
    for k in range(CONV):
        pair = map_taps[k, :, map_cols].astype(f32)
        weight_b.append(pair[0:1])
        weight_c.append(pair[1:2])
        taps[k : k + 1, width : width + bc] = pair[0:1]
        taps[k : k + 1, width + bc :] = pair[1:2]
    direct_half = pick(direct[...], tp, n_tp, heads)
    vectors[0:1, :] = spread(direct_half, heads)
    gain_rows[...] = norm_gain[...].astype(f32)
    per_row = width // LANES
    for j in range(per_row):
        vectors[1:2, j * LANES : (j + 1) * LANES] = gain_rows[pl.ds(tp * per_row + j, 1), :]
    small[0:1, :heads] = pick(bias[...], tp, n_tp, heads)
    small[1:2, :heads] = pick(speed[...], tp, n_tp, heads)

    for s in range(own):
        a = acc[s]
        xs, bs, cs = [], [], []
        for k in range(keep):
            row = heads_window[a + k].astype(f32)
            xs.append(row[s : s + 1])
            pair = maps_window[s, a + k]
            tail_maps[s, k] = pair
            pair = pair.astype(f32)
            bs.append(pair[0:1])
            cs.append(pair[1:2])
        for k in range(keep):
            tail_x[k, s : s + 1, :] = xs[k].astype(bf16)
        for at, weights, rows in (
            (0, [weight_x[k : k + 1] for k in range(CONV)], xs),
            (width, weight_b, bs),
            (width + bc, weight_c, cs),
        ):
            size = rows[0].shape[1]
            for t in range(props):
                total = jnp.zeros((1, size), f32)
                for k in range(CONV):
                    if t + k < keep:
                        total = total + weights[k] * rows[t + k]
                conv_tail[s * props + t : s * props + t + 1, at : at + size] = total

        logs = past_logs[s]
        after = jnp.zeros((1, heads), f32)
        coefficients = [None] * props
        for j in reversed(range(props)):
            coefficients[j] = jnp.where(j < a, jnp.exp(after), 0.0)
            after = after + jnp.where(j < a, logs[j : j + 1], 0.0)
        factor = jnp.exp(after)
        coefficient = spread(jnp.concatenate(coefficients, axis=0), heads)
        scaled = past_x[s].astype(f32) * coefficient
        high = scaled.astype(bf16).astype(f32)
        left = jnp.concatenate([high, scaled - high], axis=0)
        maps = past_maps[s].astype(f32)
        maps = jnp.concatenate([maps, maps], axis=0).astype(bf16)
        for g in range(groups):
            block = left[:, g * group_width : (g + 1) * group_width]
            update = lax.dot_general(
                block.astype(bf16),
                maps[:, g * STATE : (g + 1) * STATE],
                TN,
                preferred_element_type=f32,
            )
            for i in range(per_group):
                h = g * per_group + i
                value = state[s, h] * factor[:, h : h + 1]
                value = value + update[i * HEAD_DIM : (i + 1) * HEAD_DIM]
                new_state[s, h] = value
                state_low[s, h * HEAD_DIM : (h + 1) * HEAD_DIM, :] = value.astype(bf16)


def mixer_kernel(
    n_features,
    n_blocks,
    decay_total,
    state_low,
    conv_tail,
    taps,
    vectors,
    small,
    *rest,
):
    blocks = rest[:n_blocks]
    normed, raw_out, weighted_out, maps_out, logs_out = rest[n_blocks:]
    own, _, heads = decay_total.shape
    rows, width = weighted_out.shape
    props = rows // own
    bc = (conv_tail.shape[1] - width) // 2
    groups = bc // STATE
    group_width = width // groups
    total = None
    for block in blocks:
        for piece in [block[...]] if len(block.shape) == 2 else [block[i] for i in range(block.shape[0])]:
            piece = piece.astype(f32)
            total = piece if total is None else total + piece
    conv_width = width + 2 * bc
    tail = total[:, conv_width + width :]
    squares = tail[:, heads : heads + 1] + tail[:, heads + 1 : heads + 2]
    inv_rms = lax.rsqrt(squares / n_features + eps)
    raw = (total[:, :conv_width] * inv_rms).astype(bf16)
    raw_out[...] = raw
    raw = raw.astype(f32)
    gate = total[:, conv_width : conv_width + width] * inv_rms

    step_pre = tail[:, :heads] * inv_rms + small[0:1, :heads]
    step = jnp.maximum(step_pre, 0.0) + jnp.log1p(jnp.exp(-jnp.abs(step_pre)))
    totals = jnp.concatenate([decay_total[s] for s in range(own)], axis=0)
    logs = totals - small[1:2, :heads] * step
    logs_out[...] = logs
    step = spread(step, heads)
    decay = spread(jnp.exp(logs), heads)

    def turn(value, d):
        return pltpu.roll(value, d, 0)

    def since(size):
        return lax.rem(lax.broadcasted_iota(jnp.int32, (rows, size), 0), props)

    pos = since(conv_width)
    conv = conv_tail[...] + taps[CONV - 1 : CONV] * raw
    for d in range(1, CONV):
        conv = conv + jnp.where(pos >= d, taps[CONV - 1 - d : CONV - d] * turn(raw, d), 0.0)
    conv = silu(conv)
    x_conv = conv[:, :width]
    b_conv = conv[:, width : width + bc]
    c_conv = conv[:, width + bc :]
    maps_out[...] = b_conv
    weighted = step * x_conv
    weighted_out[...] = weighted

    pos = since(width)
    c_low = c_conv.astype(bf16)
    row_seq = lax.broadcasted_iota(jnp.int32, (rows, group_width), 0) // props
    from_state = []
    for g in range(groups):
        left = c_low[:, g * STATE : (g + 1) * STATE]
        out = None
        for s in range(own):
            part = lax.dot_general(
                left,
                state_low[s, g * group_width : (g + 1) * group_width, :],
                NT,
                preferred_element_type=f32,
            )
            out = part if out is None else jnp.where(row_seq >= s, part, out)
        from_state.append(out)
    from_state = jnp.concatenate(from_state, axis=1)

    span = decay
    to_start = decay
    heads_out = vectors[0:1] * x_conv
    for d in range(props):
        product = c_conv * (b_conv if d == 0 else turn(b_conv, d))
        scores = jnp.concatenate(
            [
                jnp.broadcast_to(
                    jnp.sum(product[:, g * STATE : (g + 1) * STATE], axis=1, keepdims=True),
                    (rows, group_width),
                )
                for g in range(groups)
            ],
            axis=1,
        )
        if d == 0:
            heads_out = heads_out + scores * weighted
        else:
            term = scores * span * turn(weighted, d)
            heads_out = heads_out + jnp.where(pos >= d, term, 0.0)
            span = span * turn(decay, d)
            to_start = jnp.where(pos >= d, span, to_start)
    heads_out = heads_out + to_start * from_state
    gated = heads_out * silu(gate)
    for g in range(groups):
        lanes = slice(g * group_width, (g + 1) * group_width)
        part = gated[:, lanes]
        mean = jnp.sum(part * part, axis=1, keepdims=True) / group_width
        normed[:, lanes] = (part * lax.rsqrt(mean + eps) * vectors[1:2, lanes]).astype(bf16)


def outputs_kernel(
    raw, weighted, maps, logs, tail_x, tail_maps, head_input, input_maps, log_decays, heads_window, maps_window
):
    own, props, width = head_input.shape
    bc = input_maps.shape[2]
    keep = CONV - 1
    heads_window[:keep] = tail_x[...]
    rows = raw[...].astype(f32)
    weighted, maps, logs = weighted[...], maps[...], logs[...]
    for s in range(own):
        mine = slice(s * props, (s + 1) * props)
        head_input[s] = weighted[mine].astype(bf16)
        input_maps[s] = maps[mine].astype(bf16)
        log_decays[s] = logs[mine]
        maps_window[s, :keep] = tail_maps[s]
        for t in range(props):
            r = s * props + t
            pair = [rows[r : r + 1, width : width + bc], rows[r : r + 1, width + bc :]]
            maps_window[s, keep + t] = jnp.concatenate(pair, axis=0).astype(bf16)
    for t in range(props):
        both = [rows[s * props + t : s * props + t + 1, :width] for s in range(own)]
        heads_window[keep + t] = jnp.concatenate(both, axis=0).astype(bf16)


def mix_kernel(n_kv, weight, *rest):
    blocks, out = rest[:-1], rest[-1]
    kv = lax.axis_index("kv")
    _, props, _ = out.shape
    pieces = []
    for block in blocks:
        pieces += [block[...]] if len(block.shape) == 2 else [block[i] for i in range(block.shape[0])]
    rows = pieces[0].shape[0]
    own = rows // props
    left = jnp.concatenate([piece.astype(f32) for piece in pieces], axis=0).astype(bf16)
    part = jnp.dot(left, weight[...], preferred_element_type=f32)
    for k in range(n_kv):
        start = peer(kv, k, n_kv, back=True) * own
        for s in range(own):
            at = k * rows + s * props
            out[start + s] = part[at : at + props].astype(bf16)


def local(
    tokens,
    input_norm_gain,
    head_input_weight,
    output_gate_weight,
    state_maps_weight,
    step_size_weight,
    step_size_bias,
    head_decay_speed,
    proposal_decay_total,
    head_input_kernel,
    state_maps_kernel,
    head_direct_gain,
    grouped_norm_gain,
    output_weight,
    prior_state_value,
    previous_head_input,
    previous_input_maps,
    previous_log_decays,
    prior_heads_window,
    prior_maps_window,
    accepted,
):
    n_kv, n_tp = lax.axis_size("kv"), lax.axis_size("tp")
    kv, tp = lax.axis_index("kv"), lax.axis_index("tp")
    seqs, props, local_d = tokens.shape
    heads = step_size_weight.shape[1] // n_tp
    width = head_input_weight.shape[1]
    bc = state_maps_weight.shape[2]
    own = prior_state_value.shape[0]
    rows = own * props
    conv_width = width + 2 * bc
    packed = conv_width + width + LANES
    sds = jax.ShapeDtypeStruct
    vmem = pl.BlockSpec(memory_space=pltpu.VMEM)

    gain = lax.dynamic_slice_in_dim(input_norm_gain, kv * local_d, local_d, 0)
    gain = gain.astype(f32).reshape(1, local_d)
    step_part = lax.dynamic_slice(
        step_size_weight.T, (tp * heads, kv * local_d), (heads, local_d)
    )
    step_part = jnp.pad(step_part, ((0, LANES - heads), (0, 0)))
    sent = pl.pallas_call(
        functools.partial(project_kernel, n_kv, heads),
        out_shape=[sds((rows, packed), bf16)] * n_kv,
        compiler_params=params(8),
        name="project",
    )(
        tokens,
        gain,
        head_input_weight,
        state_maps_weight.reshape(local_d, 2 * bc),
        output_gate_weight,
        step_part,
    )
    if n_kv <= DIRECT:
        got = [permute(sent[k], "kv", k, n_kv) for k in reversed(range(1, n_kv))]
        got = [sent[0]] + got
    else:
        got = [lax.all_to_all(jnp.stack(sent), "kv", 0, 0)]

    (
        accepted_state,
        state_low,
        tail_x,
        tail_maps,
        conv_tail,
        taps,
        vectors,
        small,
    ) = pl.pallas_call(
        functools.partial(state_kernel, n_tp),
        out_shape=[
            sds(prior_state_value.shape, f32),
            sds((own, width, STATE), bf16),
            sds((CONV - 1, own, width), bf16),
            sds((own, CONV - 1, 2, bc), bf16),
            sds((rows, conv_width), f32),
            sds((CONV, conv_width), f32),
            sds((2, width), f32),
            sds((2, LANES), f32),
        ],
        in_specs=[pl.BlockSpec(memory_space=pltpu.SMEM)] + [vmem] * 12,
        scratch_shapes=[pltpu.VMEM((n_tp * width // LANES, LANES), f32)],
        compiler_params=params(12),
        name="state",
    )(
        accepted,
        prior_state_value,
        previous_head_input,
        previous_input_maps,
        previous_log_decays,
        jnp.transpose(prior_heads_window, (1, 0, 2)),
        prior_maps_window,
        head_input_kernel,
        state_maps_kernel,
        step_size_bias.reshape(1, -1),
        head_decay_speed.reshape(1, -1),
        head_direct_gain.reshape(1, -1),
        grouped_norm_gain.reshape(-1, LANES),
    )

    normed, raw, weighted, maps, logs = pl.pallas_call(
        functools.partial(mixer_kernel, local_d * n_kv, len(got)),
        out_shape=[
            sds((rows, width), bf16),
            sds((rows, conv_width), bf16),
            sds((rows, width), f32),
            sds((rows, bc), f32),
            sds((rows, heads), f32),
        ],
        compiler_params=params(8),
        name="mixer",
    )(proposal_decay_total, state_low, conv_tail, taps, vectors, small, *got)

    if n_kv <= DIRECT:
        gathered = [permute(normed, "kv", k, n_kv) for k in reversed(range(1, n_kv))]
        gathered = [normed] + gathered[::-1]
    else:
        gathered = [lax.all_gather(normed, "kv")]

    head_input, input_maps, log_decays, heads_window, maps_window = pl.pallas_call(
        outputs_kernel,
        out_shape=[
            sds((own, props, width), bf16),
            sds((own, props, bc), bf16),
            sds((own, props, heads), f32),
            sds((CONV - 1 + props, own, width), bf16),
            sds((own, CONV - 1 + props, 2, bc), bf16),
        ],
        compiler_params=params(8),
        name="outputs",
    )(raw, weighted, maps, logs, tail_x, tail_maps)

    part = pl.pallas_call(
        functools.partial(mix_kernel, n_kv),
        out_shape=sds((seqs, props, local_d), bf16),
        compiler_params=params(8),
        name="mix",
    )(output_weight, *gathered)
    total = part.astype(f32)
    for k in range(1, n_tp):
        total = total + permute(part, "tp", k, n_tp).astype(f32)
    return (
        total.astype(bf16),
        accepted_state,
        head_input,
        input_maps,
        log_decays,
        jnp.transpose(heads_window, (1, 0, 2)),
        maps_window,
    )


def solution(mesh):
    return jax.shard_map(
        local,
        mesh=mesh,
        in_specs=(
            P("dp", None, "kv"),
            P(),
            P("kv", "tp"),
            P("kv", "tp"),
            P("kv", None, "tp"),
            P(),
            P(),
            P(),
            P(("dp", "kv"), None, "tp"),
            P(),
            P(),
            P(),
            P(),
            P("tp", "kv"),
            P(("dp", "kv"), "tp", None, None),
            P(("dp", "kv"), None, "tp"),
            P(("dp", "kv"), None, "tp"),
            P(("dp", "kv"), None, "tp"),
            P(("dp", "kv"), None, "tp"),
            P(("dp", "kv"), None, None, "tp"),
            P(("dp", "kv")),
        ),
        out_specs=(
            P("dp", None, "kv"),
            P(("dp", "kv"), "tp", None, None),
            P(("dp", "kv"), None, "tp"),
            P(("dp", "kv"), None, "tp"),
            P(("dp", "kv"), None, "tp"),
            P(("dp", "kv"), None, "tp"),
            P(("dp", "kv"), None, None, "tp"),
        ),
        check_vma=False,
    )
```

time: 89.1 us -> 26.9 us (0.30)
  blocking collectives: 39.4 us -> 0 us
  between operations: 14.5 us -> 0.88 us
  other arithmetic: 12.5 us -> 1.4 us
  matrix products: 10.3 us -> 0 us
  starting transfers between devices: 0.04 us -> 10.2 us
  Pallas kernels: 0 us -> 5.15 us
  local copies, waits for them, and re-layouts: 4.94 us -> 3.12 us
  waiting for transfers between devices: 6.89 us -> 5.96 us
    psum x3 -> x0, blocking collectives: 26.1 us -> none  [the longest x1 13.6 us: local(): row_total = lax.psum(sumsq, 'kv')]
    all_gather x1 -> x0, blocking collectives: 13.3 us -> none  [local(): lax.all_gather(flat, 'kv', axis=0, tiled=True)]
    dot_general x10 -> x0, matrix products: 10.3 us -> none  [the longest x1 2.54 us: local_mixer_output(): jnp.einsum('sthn,shpn->sthp', c_heads, carried, precision=lax.Precision.H...]
    ppermute x0 -> x7, starting transfers between devices: none -> 10.2 us  [permute(): lax.ppermute(array, axis, [(i, int(peer(i, k, n))) for i in range(n)])]
    psum x1 -> x0, waiting for transfers between devices: 6.87 us -> none  [local(): lax.psum(shortened(members), 'kv')]
    ppermute x0 -> x7, waiting for transfers between devices: none -> 5.96 us  [permute(): lax.ppermute(array, axis, [(i, int(peer(i, k, n))) for i in range(n)])]
    convert_element_type x11 -> x1, other arithmetic: 6.16 us -> 0.63 us  [local(): total.astype(bf16)]
    pallas_call x0 -> x5, Pallas kernels: none -> 5.15 us  [the longest x1 2.64 us: local(): pl.pallas_call(functools.partial(state_kernel, n_tp), out_shape=[sds(prio...]
  transfers between devices with their start and end apart: 1 -> 7, of which waited for: 1 -> 4; matrix products, arithmetic and copies ran while one was open for 11% -> 0% of each run, Pallas kernels for 0% -> 12%
where the time goes in v1:
time: 26.9 us; the launch traced here: 26.7 us
  starting transfers between devices  10.2 us (38%)
  waiting for transfers between devices  5.96 us (22%)
  Pallas kernels  5.15 us (19%)
  local copies, waits for them, and re-layouts  3.12 us (12%)
  other arithmetic  1.4 us (5%)
  between operations  0.88 us (3%)
    ppermute x7, starting transfers between devices, permute(): lax.ppermute(array, axis, [(i, int(peer(i, k, n))) for i in range(n)])  10.2 us
    ppermute x7, waiting for transfers between devices, permute(): lax.ppermute(array, axis, [(i, int(peer(i, k, n))) for i in range(n)])  5.96 us
    unnamed x39, local copies, waits for them, and re-layouts  3.1 us
    pallas_call x1, Pallas kernels, local(): pl.pallas_call(functools.partial(state_kernel, n_tp), out_shape=[sds(prio...  2.64 us
    pallas_call x1, Pallas kernels, local(): pl.pallas_call(functools.partial(project_kernel, n_kv, heads), out_shape=...  0.86 us
    reshape x1, other arithmetic, local(): gain = gain.astype(f32).reshape(1, local_d)  0.76 us
    pallas_call x1, Pallas kernels, local(): pl.pallas_call(outputs_kernel, out_shape=[sds((own, props, width), bf16),...  0.67 us
    convert_element_type x1, other arithmetic, local(): total.astype(bf16)  0.63 us
  transfers between devices with their start and end apart: 7, of which 4 were waited for; matrix products, arithmetic and copies ran while one was open for 0% of the time, Pallas kernels for 12%

profile of v1, /device:TPU:0, one launch (start us, length us, event | category | flops | bytes accessed | tf_op | source)
XLA Modules:
  0.0 26.7 jit_solution(8432985900407255065)
XLA Ops:
  0.6 0.0 copy-start
  0.6 0.0 copy-start.3
  0.7 0.0 copy-start.6
  0.7 1.6 %copy.28 = bf16[64,8,2,512]{3,1,2,0:T(8,128)(2,1)S(1)} copy(bf16[64,8,2,512]{3,2,1,0:T(2,128)(2,1)} %bitcast.18) | data formatting | bytes 2097152
  2.3 0.8 %dynamic-slice_convert_fusion = f32[512]{0:T(512)S(1)} fusion(bf16[2048]{0:T(1024)(128)(2,1)} %param.22, s32[]{:T(128)S(6)} %select_n.7), kind=kLoop, calls=%fused_computation.2 | loop fusion | flops 512 | bytes 3076 | tf_op jit(solution)/shard_map/reshape | solution.py:390
  3.0 0.0 copy-done
  3.1 0.0 copy-done.3
  3.1 0.0 copy-done.6
  3.1 0.0 copy-start.4
  3.1 1.4 %copy-done.4 = bf16[512,1536]{1,0:T(8,128)(2,1)S(1)} copy-done((bf16[512,1536]{1,0:T(8,128)(2,1)S(1)}, bf16[512,1536]{1,0:T(8,128)(2,1)}, u32[]{:S(2)}) %copy-start.4) | copy-done | bytes 1572888
  4.5 0.0 copy-start.9
  4.5 0.0 copy-start.10
  4.5 0.0 copy-start.11
  4.5 0.0 copy-start.12
  4.5 0.0 copy-start.13
  4.6 0.0 copy-start.15
  4.6 0.0 copy-start.16
  4.6 0.0 copy-start.17
  4.6 0.0 copy-start.18
  4.6 0.9 %project.1 = (bf16[8,4224]{1,0:T(8,128)(2,1)S(1)}, bf16[8,4224]{1,0:T(8,128)(2,1)S(1)}, bf16[8,4224]{1,0:T(8,128)(2,1)S(1)}, bf16[8,4224]{1,0:T(8,128)(2,1)S(1)}) custom-call(bf16[8,4,512]{2,1,0:T(4,128)(2,1)S(1)} %copy-done.6, f32[1,512]{1,0:T(1,128)S(1)} %bitcast.13, bf16[512,1536]{1,0:T(8,128)(2,1)S(1)} %copy-done.3, bf16[512,1024]{1,0:T(8,128)(2,1)S(1)} %bitcast.11, ...), custom_call_target="tpu_custom_call" | custom-call | tf_op jit(solution)/shard_map/project/pallas_call | solution.py:395
  5.5 0.0 copy-start.2
  5.5 5.1 %collective-permute-start = (bf16[8,4224]{1,0:T(8,128)(2,1)S(1)}, bf16[8,4224]{1,0:T(8,128)(2,1)S(1)}, u32[]{:S(2)}, u32[]{:S(2)}) collective-permute-start(bf16[8,4224]{1,0:T(8,128)(2,1)S(1)} %get-tuple-element.35), channel_id=1, source_target_pairs={{0,6},{2,4},{4,2},{6,0},{1,7},{3,5},{5,3},{7,1},{8,14},{10,12},{12... | collective-permute-start | bytes 202760 | tf_op jit(solution)/shard_map/ppermute | solution.py:37
  10.6 0.0 collective-permute-start.1
  10.6 0.6 %collective-permute-start.2 = (bf16[8,4224]{1,0:T(8,128)(2,1)S(1)}, bf16[8,4224]{1,0:T(8,128)(2,1)S(1)}, u32[]{:S(2)}, u32[]{:S(2)}) collective-permute-start(bf16[8,4224]{1,0:T(8,128)(2,1)S(1)} %get-tuple-element.37), channel_id=1, source_target_pairs={{0,2},{2,0},{4,6},{6,4},{1,3},{3,1},{5,7},{7,5},{8,10},{10,8},{12,... | collective-permute-start | bytes 202760 | tf_op jit(solution)/shard_map/ppermute | solution.py:37
  11.3 0.0 copy-done.1
  11.3 0.0 copy-done.5
  11.3 0.0 copy-done.7
  11.3 0.0 copy-done.8
  11.3 0.0 copy-done.9
  11.3 0.0 copy-done.10
  11.3 0.0 copy-done.11
  11.4 2.6 %state.2 = (f32[2,24,64,128]{3,2,1,0:T(8,128)}, bf16[2,1536,128]{2,1,0:T(8,128)(2,1)S(1)}, bf16[3,2,1536]{2,1,0:T(2,128)(2,1)S(1)}, bf16[2,3,2,512]{3,2,1,0:T(2,...) custom-call(s32[2]{0:T(128)S(1)} %copy-done.15, ...), custom_call_target="tpu_custom_call" | custom-call | tf_op jit(solution)/shard_map/state/pallas_call | solution.py:423
  14.0 0.0 collective-permute-done.rest_1_
  14.0 2.4 %collective-permute-done.1.rest_2_ = bf16[8,4224]{1,0:T(8,128)(2,1)S(1)} collective-permute-done((bf16[8,4224]{1,0:T(8,128)(2,1)S(1)}, bf16[8,4224]{1,0:T(8,128)(2,1)S(1)}, u32[]{:S(2)}, u32[]{:S(2)}) %collective-permute-start.1) | collective-permute-done | bytes 67616 | tf_op jit(solution)/shard_map/ppermute | solution.py:37
  16.4 0.0 collective-permute-done.2.rest_3_
  16.4 0.6 %mixer.1 = (bf16[8,1536]{1,0:T(8,128)(2,1)S(1)}, bf16[8,2560]{1,0:T(8,128)(2,1)S(1)}, f32[8,1536]{1,0:T(8,128)S(1)}, f32[8,512]{1,0:T(8,128)S(1)}, f32[8,24]{1,0:T(8,128)S(1)}) custom-call(f32[2,4,24]{2,1,0:T(4,128)S(1)} %copy-done.14, bf16[2,1536,128]{2,1,0:T(8,128)(2,1)S(1)} %get-tuple-element.29.state_low, f32[8,2560]{1,0:T(8,128)S(1)} %get-tuple-element.30.conv_tail, ...), custom_call_target="tpu_custom_call" | custom-call | tf_op jit(solution)/shard_map/mixer/pallas_call | solution.py:455
  17.0 2.7 %collective-permute-start.5 = (bf16[8,1536]{1,0:T(8,128)(2,1)S(1)}, bf16[8,1536]{1,0:T(8,128)(2,1)S(1)}, u32[]{:S(2)}, u32[]{:S(2)}) collective-permute-start(bf16[8,1536]{1,0:T(8,128)(2,1)S(1)} %get-tuple-element.38.rest_0_), channel_id=1, source_target_pairs={{0,6},{2,4},{4,2},{6,0},{1,7},{3,5},{5,3},{7,1},{8,14},{10,12},{12... | collective-permute-start | bytes 73736 | tf_op jit(solution)/shard_map/ppermute | solution.py:37
  19.7 0.0 collective-permute-start.4
  19.7 1.7 %collective-permute-start.3 = (bf16[8,1536]{1,0:T(8,128)(2,1)S(1)}, bf16[8,1536]{1,0:T(8,128)(2,1)S(1)}, u32[]{:S(2)}, u32[]{:S(2)}) collective-permute-start(bf16[8,1536]{1,0:T(8,128)(2,1)S(1)} %get-tuple-element.38.rest_0_), channel_id=1, source_target_pairs={{0,2},{2,0},{4,6},{6,4},{1,3},{3,1},{5,7},{7,5},{8,10},{10,8},{12,... | collective-permute-start | bytes 73736 | tf_op jit(solution)/shard_map/ppermute | solution.py:37
  21.4 1.2 %collective-permute-done.5.rest_3_ = bf16[8,1536]{1,0:T(8,128)(2,1)S(1)} collective-permute-done((bf16[8,1536]{1,0:T(8,128)(2,1)S(1)}, bf16[8,1536]{1,0:T(8,128)(2,1)S(1)}, u32[]{:S(2)}, u32[]{:S(2)}) %collective-permute-start.5) | collective-permute-done | bytes 24608 | tf_op jit(solution)/shard_map/ppermute | solution.py:37
  22.7 1.8 %collective-permute-done.4.rest_2_ = bf16[8,1536]{1,0:T(8,128)(2,1)S(1)} collective-permute-done((bf16[8,1536]{1,0:T(8,128)(2,1)S(1)}, bf16[8,1536]{1,0:T(8,128)(2,1)S(1)}, u32[]{:S(2)}, u32[]{:S(2)}) %collective-permute-start.4) | collective-permute-done | bytes 24608 | tf_op jit(solution)/shard_map/ppermute | solution.py:37
  24.5 0.0 collective-permute-done.3.rest_1_
  24.5 0.0 copy-done.2
  24.5 0.4 %mix.1 = bf16[8,4,512]{2,1,0:T(4,128)(2,1)S(1)} custom-call(bf16[1536,512]{1,0:T(8,128)(2,1)S(1)} %copy-done.2, bf16[8,1536]{1,0:T(8,128)(2,1)S(1)} %get-tuple-element.38.rest_0_, bf16[8,1536]{1,0:T(8,128)(2,1)S(1)} %collective-permute-done.3.rest_1_, bf16[8,1536]{1,0:T(8,128)(2,1)S(1)} %collective-permute-done.4.rest_2_, ...), custom_call_target="tpu_custom_call" | custom-call | tf_op jit(solution)/shard_map/mix/pallas_call | solution.py:487
  24.8 0.0 collective-permute-start.6
  24.9 0.7 %outputs.1 = (bf16[2,4,1536]{2,1,0:T(4,128)(2,1)}, bf16[2,4,512]{2,1,0:T(4,128)(2,1)}, f32[2,4,24]{2,1,0:T(4,128)}, bf16[7,2,1536]{2,1,0:T(2,128)(2,1)}, bf16[2,7,2,512]{3,2,1,0:T(2,128)(2,1)}) custom-call(bf16[8,2560]{1,0:T(8,128)(2,1)S(1)} %get-tuple-element.40.raw, f32[8,1536]{1,0:T(8,128)S(1)} %get-tuple-element.41.weighted, ...), custom_call_target="tpu_custom_call" | custom-call | tf_op jit(solution)/shard_map/outputs/pallas_call | solution.py:474
  25.5 0.5 %collective-permute-done.6 = bf16[8,4,512]{2,1,0:T(4,128)(2,1)S(1)} collective-permute-done((bf16[8,4,512]{2,1,0:T(4,128)(2,1)S(1)}, bf16[8,4,512]{2,1,0:T(4,128)(2,1)S(1)}, u32[]{:S(2)}, u32[]{:S(2)}) %collective-permute-start.6) | collective-permute-done | bytes 32800 | tf_op jit(solution)/shard_map/ppermute | solution.py:37
  26.1 0.6 %add_convert_fusion = bf16[8,4,512]{2,1,0:T(4,128)(2,1)} fusion(bf16[8,4,512]{2,1,0:T(4,128)(2,1)S(1)} %collective-permute-done.6, bf16[8,4,512]{2,1,0:T(4,128)(2,1)S(1)} %mix.1), kind=kLoop, calls=%fused_computation | loop fusion | flops 65536 | bytes 98304 | tf_op jit(solution)/shard_map/convert_element_type | solution.py:497
  (14 shorter events, 0.0 us)
Async XLA Ops:
  0.6 2.4 %copy-start = (bf16[2048,48]{0,1:T(8,128)(2,1)S(1)}, bf16[2048,48]{0,1:T(8,128)(2,1)}, u32[]{:S(2)}) copy-start(bf16[2048,48]{0,1:T(8,128)(2,1)} %param.26) | copy-start | bytes 589828
  0.6 2.4 %copy-start.3 = (bf16[512,1536]{1,0:T(8,128)(2,1)S(1)}, bf16[512,1536]{1,0:T(8,128)(2,1)}, u32[]{:S(2)}) copy-start(bf16[512,1536]{1,0:T(8,128)(2,1)} %wx.1) | copy-start | bytes 4718596
  0.7 2.4 %copy-start.6 = (bf16[8,4,512]{2,1,0:T(4,128)(2,1)S(1)}, bf16[8,4,512]{2,1,0:T(4,128)(2,1)}, u32[]{:S(2)}) copy-start(bf16[8,4,512]{2,1,0:T(4,128)(2,1)} %tok.1) | copy-start | bytes 98308
  3.1 1.4 %copy-start.4 = (bf16[512,1536]{1,0:T(8,128)(2,1)S(1)}, bf16[512,1536]{1,0:T(8,128)(2,1)}, u32[]{:S(2)}) copy-start(bf16[512,1536]{1,0:T(8,128)(2,1)} %wg.1) | copy-start | bytes 4718596
  4.5 6.8 %copy-start.1 = (f32[2,24,64,128]{3,2,1,0:T(8,128)S(1)}, f32[2,24,64,128]{3,2,1,0:T(8,128)}, u32[]{:S(2)}) copy-start(f32[2,24,64,128]{3,2,1,0:T(8,128)} %state.3) | copy-start | bytes 4718596
  4.5 6.8 %copy-start.5 = (bf16[2,7,1536]{2,0,1:T(2,128)(2,1)S(1)}, bf16[2,7,1536]{2,0,1:T(2,128)(2,1)}, u32[]{:S(2)}) copy-start(bf16[2,7,1536]{2,0,1:T(2,128)(2,1)} %param.39) | copy-start | bytes 129028
  4.5 6.8 %copy-start.7 = (bf16[2,7,2,512]{3,2,1,0:T(2,128)(2,1)S(1)}, bf16[2,7,2,512]{3,2,1,0:T(2,128)(2,1)}, u32[]{:S(2)}) copy-start(bf16[2,7,2,512]{3,2,1,0:T(2,128)(2,1)} %maps_window.1) | copy-start | bytes 86020
  4.5 6.8 %copy-start.8 = (bf16[2,4,1536]{2,1,0:T(4,128)(2,1)S(1)}, bf16[2,4,1536]{2,1,0:T(4,128)(2,1)}, u32[]{:S(2)}) copy-start(bf16[2,4,1536]{2,1,0:T(4,128)(2,1)} %past_x.1) | copy-start | bytes 73732
  4.5 6.8 %copy-start.9 = (bf16[4,3072]{1,0:T(4,128)(2,1)S(1)}, bf16[4,3072]{1,0:T(4,128)(2,1)}, u32[]{:S(2)}) copy-start(bf16[4,3072]{1,0:T(4,128)(2,1)} %head_taps.1) | copy-start | bytes 73732
  4.5 6.8 %copy-start.10 = (bf16[4,2,1024]{2,1,0:T(2,128)(2,1)S(1)}, bf16[4,2,1024]{2,1,0:T(2,128)(2,1)}, u32[]{:S(2)}) copy-start(bf16[4,2,1024]{2,1,0:T(2,128)(2,1)} %map_taps.1) | copy-start | bytes 49156
  4.5 6.8 %copy-start.11 = (bf16[2,4,512]{2,1,0:T(4,128)(2,1)S(1)}, bf16[2,4,512]{2,1,0:T(4,128)(2,1)}, u32[]{:S(2)}) copy-start(bf16[2,4,512]{2,1,0:T(4,128)(2,1)} %past_maps.1) | copy-start | bytes 24580
  4.5 6.8 %copy-start.12 = (bf16[3072]{0:T(1024)(128)(2,1)S(1)}, bf16[3072]{0:T(1024)(128)(2,1)}, u32[]{:S(2)}) copy-start(bf16[3072]{0:T(1024)(128)(2,1)} %param.33) | copy-start | bytes 18436
  4.5 6.8 %copy-start.13 = (f32[2,4,24]{2,1,0:T(4,128)S(1)}, f32[2,4,24]{2,1,0:T(4,128)}, u32[]{:S(2)}) copy-start(f32[2,4,24]{2,1,0:T(4,128)} %past_logs.1) | copy-start | bytes 2308
  4.6 6.8 %copy-start.15 = (s32[2]{0:T(128)S(1)}, s32[2]{0:T(128)}, u32[]{:S(2)}) copy-start(s32[2]{0:T(128)} %acc.1) | copy-start | bytes 28
  4.6 6.8 %copy-start.16 = (f32[48]{0:T(128)S(1)}, f32[48]{0:T(128)}, u32[]{:S(2)}) copy-start(f32[48]{0:T(128)} %param.27) | copy-start | bytes 580
  4.6 6.8 %copy-start.17 = (f32[48]{0:T(128)S(1)}, f32[48]{0:T(128)}, u32[]{:S(2)}) copy-start(f32[48]{0:T(128)} %param.28) | copy-start | bytes 580
  4.6 6.8 %copy-start.18 = (f32[48]{0:T(128)S(1)}, f32[48]{0:T(128)}, u32[]{:S(2)}) copy-start(f32[48]{0:T(128)} %param.32) | copy-start | bytes 580
  5.5 10.9 %copy-start.14 = (f32[2,4,24]{2,1,0:T(4,128)S(1)}, f32[2,4,24]{2,1,0:T(4,128)}, u32[]{:S(2)}) copy-start(f32[2,4,24]{2,1,0:T(4,128)} %decay_total.1) | copy-start | bytes 2308
  5.5 19.0 %copy-start.2 = (bf16[1536,512]{1,0:T(8,128)(2,1)S(1)}, bf16[1536,512]{1,0:T(8,128)(2,1)}, u32[]{:S(2)}) copy-start(bf16[1536,512]{1,0:T(8,128)(2,1)} %weight.1) | copy-start | bytes 4718596
  5.5 8.5 %collective-permute-start = (bf16[8,4224]{1,0:T(8,128)(2,1)S(1)}, bf16[8,4224]{1,0:T(8,128)(2,1)S(1)}, u32[]{:S(2)}, u32[]{:S(2)}) collective-permute-start(bf16[8,4224]{1,0:T(8,128)(2,1)S(1)} %get-tuple-element.35), channel_id=1, source_target_pairs={{0,6},{2,4},{4,2},{6,0},{1,7},{3,5},{5,3},{7,1},{8,14},{10,12},{12... | collective-permute-start | bytes 202760 | tf_op jit(solution)/shard_map/ppermute | solution.py:37
  10.6 5.8 %collective-permute-start.1 = (bf16[8,4224]{1,0:T(8,128)(2,1)S(1)}, bf16[8,4224]{1,0:T(8,128)(2,1)S(1)}, u32[]{:S(2)}, u32[]{:S(2)}) collective-permute-start(bf16[8,4224]{1,0:T(8,128)(2,1)S(1)} %get-tuple-element.36), channel_id=1, source_target_pairs={{0,4},{2,6},{4,0},{6,2},{1,5},{3,7},{5,1},{7,3},{8,12},{10,14},{12... | collective-permute-start | bytes 202760 | tf_op jit(solution)/shard_map/ppermute | solution.py:37
  10.6 5.8 %collective-permute-start.2 = (bf16[8,4224]{1,0:T(8,128)(2,1)S(1)}, bf16[8,4224]{1,0:T(8,128)(2,1)S(1)}, u32[]{:S(2)}, u32[]{:S(2)}) collective-permute-start(bf16[8,4224]{1,0:T(8,128)(2,1)S(1)} %get-tuple-element.37), channel_id=1, source_target_pairs={{0,2},{2,0},{4,6},{6,4},{1,3},{3,1},{5,7},{7,5},{8,10},{10,8},{12,... | collective-permute-start | bytes 202760 | tf_op jit(solution)/shard_map/ppermute | solution.py:37
  17.0 5.7 %collective-permute-start.5 = (bf16[8,1536]{1,0:T(8,128)(2,1)S(1)}, bf16[8,1536]{1,0:T(8,128)(2,1)S(1)}, u32[]{:S(2)}, u32[]{:S(2)}) collective-permute-start(bf16[8,1536]{1,0:T(8,128)(2,1)S(1)} %get-tuple-element.38.rest_0_), channel_id=1, source_target_pairs={{0,6},{2,4},{4,2},{6,0},{1,7},{3,5},{5,3},{7,1},{8,14},{10,12},{12... | collective-permute-start | bytes 73736 | tf_op jit(solution)/shard_map/ppermute | solution.py:37
  19.7 4.7 %collective-permute-start.4 = (bf16[8,1536]{1,0:T(8,128)(2,1)S(1)}, bf16[8,1536]{1,0:T(8,128)(2,1)S(1)}, u32[]{:S(2)}, u32[]{:S(2)}) collective-permute-start(bf16[8,1536]{1,0:T(8,128)(2,1)S(1)} %get-tuple-element.38.rest_0_), channel_id=1, source_target_pairs={{0,4},{2,6},{4,0},{6,2},{1,5},{3,7},{5,1},{7,3},{8,12},{10,14},{12... | collective-permute-start | bytes 73736 | tf_op jit(solution)/shard_map/ppermute | solution.py:37
  19.7 4.7 %collective-permute-start.3 = (bf16[8,1536]{1,0:T(8,128)(2,1)S(1)}, bf16[8,1536]{1,0:T(8,128)(2,1)S(1)}, u32[]{:S(2)}, u32[]{:S(2)}) collective-permute-start(bf16[8,1536]{1,0:T(8,128)(2,1)S(1)} %get-tuple-element.38.rest_0_), channel_id=1, source_target_pairs={{0,2},{2,0},{4,6},{6,4},{1,3},{3,1},{5,7},{7,5},{8,10},{10,8},{12,... | collective-permute-start | bytes 73736 | tf_op jit(solution)/shard_map/ppermute | solution.py:37
  24.8 1.2 %collective-permute-start.6 = (bf16[8,4,512]{2,1,0:T(4,128)(2,1)S(1)}, bf16[8,4,512]{2,1,0:T(4,128)(2,1)S(1)}, u32[]{:S(2)}, u32[]{:S(2)}) collective-permute-start(bf16[8,4,512]{2,1,0:T(4,128)(2,1)S(1)} %mix.1), channel_id=1, source_target_pairs={{0,1},{1,0},{2,3},{3,2},{4,5},{5,4},{6,7},{7,6},{8,9},{9,8},{10,11... | collective-permute-start | bytes 98312 | tf_op jit(solution)/shard_map/ppermute | solution.py:37

commit v2 on v1

--- a/solution.py
+++ b/solution.py
@@ -62,33 +62,102 @@
     return x * (1.0 / (1.0 + jnp.exp(-x)))
 
 
-def project_kernel(n_kv, n_heads, tok, gain, wx, wm, wg, ws, *outs):
-    kv = lax.axis_index("kv")
+def project_kernel(n_kv, n_tp, chunk, tok_hbm, gain_hbm, wx, wm, wg, ws_hbm, *rest):
+    outs = rest[:n_kv]
+    tok, gain, gain_rows, ws, step_rows, wide, pairs, sems = rest[n_kv:]
+    kv, tp = lax.axis_index("kv"), lax.axis_index("tp")
     seqs, props, local_d = tok.shape
     own = seqs // n_kv
     rows = own * props
-    parts, squares = [], []
+    width, bc = wx.shape[1], wm.shape[2]
+    heads = ws.shape[0] // n_tp
+    aligned = local_d % LANES == 0
+
+    copies = []
+
+    def fetch(source, target):
+        copy = pltpu.make_async_copy(source, target, sems.at[len(copies)])
+        copy.start()
+        copies.append(copy)
+        return copy
+
+    small = [fetch(tok_hbm, tok), fetch(gain_hbm, gain)]
+    columns = pl.ds(pl.multiple_of(kv * local_d, LANES), local_d) if aligned else slice(None)
+    small.append(fetch(ws_hbm.at[:, columns], ws))
+    maps = fetch(wm, pairs)
+    plan = []
+    for at in range(0, width, chunk):
+        here = slice(at, at + chunk)
+        plan.append((fetch(wx.at[:, here], wide.at[:, here]), at, here))
+    for at in range(0, width, chunk):
+        here = slice(width + at, width + at + chunk)
+        plan.append((fetch(wg.at[:, at : at + chunk], wide.at[:, here]), width + 2 * bc + at, here))
+
+    for copy in small:
+        copy.wait()
+    parts = []
     for k in range(n_kv):
         start = peer(kv, k, n_kv) * own
         for s in range(own):
-            values = tok[start + s].astype(f32)
-            parts.append(values)
+            parts.append(tok[start + s].astype(f32))
     values = jnp.concatenate(parts, axis=0)
     squares = jnp.sum(values * values, axis=1, keepdims=True)
-    scaled = (values * gain[...]).astype(bf16)
+    gain_rows[...] = gain[...].astype(f32)
+    if aligned:
+        per = local_d // LANES
+        factor = [gain_rows[pl.ds(kv * per + j, 1), :] for j in range(per)]
+        factor = jnp.concatenate(factor, axis=1)
+    else:
+        factor = gain_rows[...]
+    scaled = values * factor
+    row = lax.broadcasted_iota(jnp.int32, (LANES, 2 * LANES), 0)
+    column = lax.broadcasted_iota(jnp.int32, (LANES, 2 * LANES), 1)
+    low = scaled.astype(bf16)
+    apart = []
+    for index in range(2):
+        place = (column == 2 * row + index).astype(f32).astype(bf16)
+        apart.append(
+            jnp.concatenate(
+                [
+                    jnp.dot(low[:, at : at + LANES], place[: min(LANES, local_d), : 2 * min(LANES, local_d)], preferred_element_type=f32)
+                    for at in range(0, local_d, LANES)
+                ],
+                axis=1,
+            )
+        )
+    apart = jnp.concatenate(apart, axis=0).astype(bf16)
+
     high = squares.astype(bf16).astype(f32)
-    step = lax.dot_general(scaled, ws[...], NT, preferred_element_type=f32)
+    step = lax.dot_general(low, ws[...], NT, preferred_element_type=f32)
+    step_rows[...] = jnp.zeros_like(step_rows)
+    step_rows[:, :heads] = pick(step, tp, n_tp, heads)
+    step = step_rows[...]
     lane = lax.broadcasted_iota(jnp.int32, step.shape, 1)
-    step = jnp.where(lane == n_heads, high, jnp.where(lane == n_heads + 1, squares - high, step))
-    at = 0
-    for block in (wx, wm, wg):
-        width = block.shape[1]
-        part = jnp.dot(scaled, block[...], preferred_element_type=f32)
+    step = jnp.where(lane == heads, high, jnp.where(lane == heads + 1, squares - high, step))
+
+    def put(at, part):
         for k in range(n_kv):
-            outs[k][:, at : at + width] = part[k * rows : (k + 1) * rows].astype(bf16)
-        at += width
-    for k in range(n_kv):
-        outs[k][:, at:] = step[k * rows : (k + 1) * rows].astype(bf16)
+            piece = part[k * rows : (k + 1) * rows].astype(bf16)
+            outs[k][:, at : at + part.shape[1]] = piece
+
+    put(2 * width + 2 * bc, step)
+    maps.wait()
+    group = 2 * LANES if bc % (2 * LANES) == 0 else LANES
+    for at in range(0, bc, group):
+        block = [
+            pairs[:, :, lane : lane + LANES].reshape(2 * local_d, LANES)
+            for lane in range(at, at + group, LANES)
+        ]
+        both = jnp.dot(apart, jnp.concatenate(block, axis=1), preferred_element_type=f32)
+        put(width + at, both[: n_kv * rows])
+        put(width + bc + at, both[n_kv * rows :])
+    count = len(plan) // 2
+    for copy, at, here in plan[:count]:
+        copy.wait()
+        put(at, jnp.dot(low, wide[:, here], preferred_element_type=f32))
+    for copy, at, here in plan[count:]:
+        copy.wait()
+        put(at, jnp.dot(low, wide[:, here], preferred_element_type=f32))
 
 
 def state_kernel(
@@ -374,7 +443,7 @@
     accepted,
 ):
     n_kv, n_tp = lax.axis_size("kv"), lax.axis_size("tp")
-    kv, tp = lax.axis_index("kv"), lax.axis_index("tp")
+    kv = lax.axis_index("kv")
     seqs, props, local_d = tokens.shape
     heads = step_size_weight.shape[1] // n_tp
     width = head_input_weight.shape[1]
@@ -386,27 +455,47 @@
     sds = jax.ShapeDtypeStruct
     vmem = pl.BlockSpec(memory_space=pltpu.VMEM)
 
-    gain = lax.dynamic_slice_in_dim(input_norm_gain, kv * local_d, local_d, 0)
-    gain = gain.astype(f32).reshape(1, local_d)
-    step_part = lax.dynamic_slice(
-        step_size_weight.T, (tp * heads, kv * local_d), (heads, local_d)
-    )
-    step_part = jnp.pad(step_part, ((0, LANES - heads), (0, 0)))
+    if local_d % LANES == 0:
+        gain = input_norm_gain.reshape(-1, LANES)
+        step_weight = step_size_weight.T
+    else:
+        gain = lax.dynamic_slice_in_dim(input_norm_gain, kv * local_d, local_d, 0)
+        gain = gain.reshape(1, local_d)
+        step_weight = lax.dynamic_slice_in_dim(step_size_weight.T, kv * local_d, local_d, 1)
+    chunk = width
+    n_copies = 3 + 2 * (width // chunk) + 1
+    hbm = pl.BlockSpec(memory_space=pltpu.HBM)
     sent = pl.pallas_call(
-        functools.partial(project_kernel, n_kv, heads),
+        functools.partial(project_kernel, n_kv, n_tp, chunk),
         out_shape=[sds((rows, packed), bf16)] * n_kv,
-        compiler_params=params(8),
+        in_specs=[hbm] * 6,
+        scratch_shapes=[
+            pltpu.VMEM(tokens.shape, bf16),
+            pltpu.VMEM(gain.shape, bf16),
+            pltpu.VMEM(gain.shape, f32),
+            pltpu.VMEM((step_weight.shape[0], local_d), bf16),
+            pltpu.VMEM((n_kv * rows, LANES), f32),
+            pltpu.VMEM((local_d, 2 * width), bf16),
+            pltpu.VMEM((local_d, 2, bc), bf16),
+            pltpu.SemaphoreType.DMA((n_copies,)),
+        ],
+        compiler_params=params(12),
         name="project",
     )(
-        tokens,
-        gain,
-        head_input_weight,
-        state_maps_weight.reshape(local_d, 2 * bc),
-        output_gate_weight,
-        step_part,
+        *(
+            pltpu.with_memory_space_constraint(array, pltpu.HBM)
+            for array in (
+                tokens,
+                gain,
+                head_input_weight,
+                state_maps_weight,
+                output_gate_weight,
+                step_weight,
+            )
+        )
     )
     if n_kv <= DIRECT:
-        got = [permute(sent[k], "kv", k, n_kv) for k in reversed(range(1, n_kv))]
+        got = [permute(sent[k], "kv", k, n_kv) for k in (2, 1, 3)]
         got = [sent[0]] + got
     else:
         got = [lax.all_to_all(jnp.stack(sent), "kv", 0, 0)]
@@ -466,8 +555,8 @@
     )(proposal_decay_total, state_low, conv_tail, taps, vectors, small, *got)
 
     if n_kv <= DIRECT:
-        gathered = [permute(normed, "kv", k, n_kv) for k in reversed(range(1, n_kv))]
-        gathered = [normed] + gathered[::-1]
+        gd = {k: permute(normed, "kv", k, n_kv) for k in (3, 2, 1)}
+        gathered = [normed] + [gd[k] for k in sorted(gd)]
     else:
         gathered = [lax.all_gather(normed, "kv")]
 

time: 26.9 us -> 24.8 us (0.922)
  local copies, waits for them, and re-layouts: 3.12 us -> 0.07 us
  Pallas kernels: 5.15 us -> 7.22 us
  other arithmetic: 1.4 us -> 0.64 us
    unnamed x39 -> x30, local copies, waits for them, and re-layouts: 3.1 us -> 0.07 us
    pallas_call x1, Pallas kernels: 0.86 us -> 2.9 us  [local(): pl.pallas_call(functools.partial(project_kernel, n_kv, n_tp, chunk), out_...]
    reshape x1 -> x0, other arithmetic: 0.76 us -> none  [local(): gain = gain.astype(f32).reshape(1, local_d)]
  transfers between devices with their start and end apart: 7 -> 7, of which waited for: 4 -> 4; matrix products, arithmetic and copies ran while one was open for 0% -> 0% of each run, Pallas kernels for 12% -> 14%
where the time goes in v2:
time: 24.8 us; the launch traced here: 24.7 us
  starting transfers between devices  10.1 us (41%)
  Pallas kernels  7.22 us (29%)
  waiting for transfers between devices  5.75 us (23%)
  between operations  0.88 us (4%)
  other arithmetic  0.64 us (3%)
    ppermute x7, starting transfers between devices, permute(): lax.ppermute(array, axis, [(i, int(peer(i, k, n))) for i in range(n)])  10.1 us
    ppermute x7, waiting for transfers between devices, permute(): lax.ppermute(array, axis, [(i, int(peer(i, k, n))) for i in range(n)])  5.75 us
    pallas_call x1, Pallas kernels, local(): pl.pallas_call(functools.partial(project_kernel, n_kv, n_tp, chunk), out_...  2.9 us
    pallas_call x1, Pallas kernels, local(): pl.pallas_call(functools.partial(state_kernel, n_tp), out_shape=[sds(prio...  2.67 us
    pallas_call x1, Pallas kernels, local(): pl.pallas_call(outputs_kernel, out_shape=[sds((own, props, width), bf16),...  0.67 us
    convert_element_type x1, other arithmetic, local(): total.astype(bf16)  0.64 us
    pallas_call x1, Pallas kernels, local(): pl.pallas_call(functools.partial(mixer_kernel, local_d * n_kv, len(got)),...  0.62 us
  transfers between devices with their start and end apart: 7, of which 4 were waited for; matrix products, arithmetic and copies ran while one was open for 0% of the time, Pallas kernels for 14%

profile of v2, /device:TPU:0, one launch (start us, length us, event | category | flops | bytes accessed | tf_op | source)
XLA Modules:
  0.0 24.7 jit_solution(13365820681461939166)
XLA Ops:
  0.6 0.0 copy-start
  0.7 0.0 copy-start.2
  0.7 0.0 copy-start.3
  0.7 0.0 copy-start.4
  0.7 0.0 copy-start.5
  0.7 0.0 copy-start.6
  0.7 0.0 copy-start.7
  0.7 0.0 copy-start.8
  0.7 0.0 copy-start.9
  0.7 0.0 copy-start.11
  0.7 0.0 copy-start.12
  0.8 0.0 copy-start.13
  0.8 0.0 copy-start.14
  0.8 2.9 %project.1 = (bf16[8,4224]{1,0:T(8,128)(2,1)S(1)}, bf16[8,4224]{1,0:T(8,128)(2,1)S(1)}, bf16[8,4224]{1,0:T(8,128)(2,1)S(1)}, bf16[8,4224]{1,0:T(8,128)(2,1)S(1)}) custom-call(bf16[8,4,512]{2,1,0:T(4,128)(2,1)} %tok_hbm.1, bf16[16,128]{1,0:T(8,128)(2,1)} %bitcast.14, bf16[512,1536]{1,0:T(8,128)(2,1)} %wx.1, bf16[512,2,512]{2,1,0:T(2,128)(2,1)} %wm.1, ...), custom_call_target="tpu_custom_call" | custom-call | tf_op jit(solution)/shard_map/project/pallas_call | solution.py:468
  3.7 0.0 copy-start.10
  3.7 0.0 copy-start.1
  3.7 4.1 %collective-permute-start = (bf16[8,4224]{1,0:T(8,128)(2,1)S(1)}, bf16[8,4224]{1,0:T(8,128)(2,1)S(1)}, u32[]{:S(2)}, u32[]{:S(2)}) collective-permute-start(bf16[8,4224]{1,0:T(8,128)(2,1)S(1)} %get-tuple-element.35), channel_id=1, source_target_pairs={{0,4},{2,6},{4,0},{6,2},{1,5},{3,7},{5,1},{7,3},{8,12},{10,14},{12... | collective-permute-start | bytes 202760 | tf_op jit(solution)/shard_map/ppermute | solution.py:37
  7.8 1.6 %collective-permute-start.1 = (bf16[8,4224]{1,0:T(8,128)(2,1)S(1)}, bf16[8,4224]{1,0:T(8,128)(2,1)S(1)}, u32[]{:S(2)}, u32[]{:S(2)}) collective-permute-start(bf16[8,4224]{1,0:T(8,128)(2,1)S(1)} %get-tuple-element.36), channel_id=1, source_target_pairs={{0,2},{2,0},{4,6},{6,4},{1,3},{3,1},{5,7},{7,5},{8,10},{10,8},{12,... | collective-permute-start | bytes 202760 | tf_op jit(solution)/shard_map/ppermute | solution.py:37
  9.4 0.0 collective-permute-start.2
  9.4 0.0 copy-done
  9.4 0.0 copy-done.2
  9.4 0.0 copy-done.3
  9.4 0.0 copy-done.4
  9.4 0.0 copy-done.5
  9.5 0.0 copy-done.6
  9.5 0.0 copy-done.7
  9.5 0.0 copy-done.8
  9.5 0.0 copy-done.9
  9.5 0.0 copy-done.11
  9.5 0.0 copy-done.12
  9.5 0.0 copy-done.13
  9.5 0.0 copy-done.14
  9.5 2.7 %state.2 = (f32[2,24,64,128]{3,2,1,0:T(8,128)}, bf16[2,1536,128]{2,1,0:T(8,128)(2,1)S(1)}, bf16[3,2,1536]{2,1,0:T(2,128)(2,1)S(1)}, bf16[2,3,2,512]{3,2,1,0:T(2,...) custom-call(s32[2]{0:T(128)S(1)} %copy-done.11, ...), custom_call_target="tpu_custom_call" | custom-call | tf_op jit(solution)/shard_map/state/pallas_call | solution.py:512
  12.2 0.0 collective-permute-done.rest_1_
  12.2 0.0 collective-permute-done.1.rest_2_
  12.2 3.3 %collective-permute-done.2.rest_3_ = bf16[8,4224]{1,0:T(8,128)(2,1)S(1)} collective-permute-done((bf16[8,4224]{1,0:T(8,128)(2,1)S(1)}, bf16[8,4224]{1,0:T(8,128)(2,1)S(1)}, u32[]{:S(2)}, u32[]{:S(2)}) %collective-permute-start.2) | collective-permute-done | bytes 67616 | tf_op jit(solution)/shard_map/ppermute | solution.py:37
  15.5 0.6 %mixer.1 = (bf16[8,1536]{1,0:T(8,128)(2,1)S(1)}, bf16[8,2560]{1,0:T(8,128)(2,1)S(1)}, f32[8,1536]{1,0:T(8,128)S(1)}, f32[8,512]{1,0:T(8,128)S(1)}, f32[8,24]{1,0:T(8,128)S(1)}) custom-call(f32[2,4,24]{2,1,0:T(4,128)S(1)} %copy-done.10, bf16[2,1536,128]{2,1,0:T(8,128)(2,1)S(1)} %get-tuple-element.29.state_low, f32[8,2560]{1,0:T(8,128)S(1)} %get-tuple-element.30.conv_tail, ...), custom_call_target="tpu_custom_call" | custom-call | tf_op jit(solution)/shard_map/mixer/pallas_call | solution.py:544
  16.1 1.3 %collective-permute-start.5 = (bf16[8,1536]{1,0:T(8,128)(2,1)S(1)}, bf16[8,1536]{1,0:T(8,128)(2,1)S(1)}, u32[]{:S(2)}, u32[]{:S(2)}) collective-permute-start(bf16[8,1536]{1,0:T(8,128)(2,1)S(1)} %get-tuple-element.38.rest_0_), channel_id=1, source_target_pairs={{0,6},{2,4},{4,2},{6,0},{1,7},{3,5},{5,3},{7,1},{8,14},{10,12},{12... | collective-permute-start | bytes 73736 | tf_op jit(solution)/shard_map/ppermute | solution.py:37
  17.5 0.2 collective-permute-start.4
  17.7 2.9 %collective-permute-start.3 = (bf16[8,1536]{1,0:T(8,128)(2,1)S(1)}, bf16[8,1536]{1,0:T(8,128)(2,1)S(1)}, u32[]{:S(2)}, u32[]{:S(2)}) collective-permute-start(bf16[8,1536]{1,0:T(8,128)(2,1)S(1)} %get-tuple-element.38.rest_0_), channel_id=1, source_target_pairs={{0,2},{2,0},{4,6},{6,4},{1,3},{3,1},{5,7},{7,5},{8,10},{10,8},{12,... | collective-permute-start | bytes 73736 | tf_op jit(solution)/shard_map/ppermute | solution.py:37
  20.5 1.2 %collective-permute-done.5.rest_3_ = bf16[8,1536]{1,0:T(8,128)(2,1)S(1)} collective-permute-done((bf16[8,1536]{1,0:T(8,128)(2,1)S(1)}, bf16[8,1536]{1,0:T(8,128)(2,1)S(1)}, u32[]{:S(2)}, u32[]{:S(2)}) %collective-permute-start.5) | collective-permute-done | bytes 24608 | tf_op jit(solution)/shard_map/ppermute | solution.py:37
  21.8 0.7 %collective-permute-done.4.rest_2_ = bf16[8,1536]{1,0:T(8,128)(2,1)S(1)} collective-permute-done((bf16[8,1536]{1,0:T(8,128)(2,1)S(1)}, bf16[8,1536]{1,0:T(8,128)(2,1)S(1)}, u32[]{:S(2)}, u32[]{:S(2)}) %collective-permute-start.4) | collective-permute-done | bytes 24608 | tf_op jit(solution)/shard_map/ppermute | solution.py:37
  22.4 0.0 collective-permute-done.3.rest_1_
  22.5 0.4 %mix.1 = bf16[8,4,512]{2,1,0:T(4,128)(2,1)S(1)} custom-call(bf16[1536,512]{1,0:T(8,128)(2,1)S(1)} %copy-done.1, bf16[8,1536]{1,0:T(8,128)(2,1)S(1)} %get-tuple-element.38.rest_0_, bf16[8,1536]{1,0:T(8,128)(2,1)S(1)} %collective-permute-done.3.rest_1_, bf16[8,1536]{1,0:T(8,128)(2,1)S(1)} %collective-permute-done.4.rest_2_, ...), custom_call_target="tpu_custom_call" | custom-call | tf_op jit(solution)/shard_map/mix/pallas_call | solution.py:576
  22.8 0.0 collective-permute-start.6
  22.8 0.7 %outputs.1 = (bf16[2,4,1536]{2,1,0:T(4,128)(2,1)}, bf16[2,4,512]{2,1,0:T(4,128)(2,1)}, f32[2,4,24]{2,1,0:T(4,128)}, bf16[7,2,1536]{2,1,0:T(2,128)(2,1)}, bf16[2,7,2,512]{3,2,1,0:T(2,128)(2,1)}) custom-call(bf16[8,2560]{1,0:T(8,128)(2,1)S(1)} %get-tuple-element.40.raw, f32[8,1536]{1,0:T(8,128)S(1)} %get-tuple-element.41.weighted, ...), custom_call_target="tpu_custom_call" | custom-call | tf_op jit(solution)/shard_map/outputs/pallas_call | solution.py:563
  23.5 0.5 %collective-permute-done.6 = bf16[8,4,512]{2,1,0:T(4,128)(2,1)S(1)} collective-permute-done((bf16[8,4,512]{2,1,0:T(4,128)(2,1)S(1)}, bf16[8,4,512]{2,1,0:T(4,128)(2,1)S(1)}, u32[]{:S(2)}, u32[]{:S(2)}) %collective-permute-start.6) | collective-permute-done | bytes 32800 | tf_op jit(solution)/shard_map/ppermute | solution.py:37
  24.0 0.6 %add_convert_fusion = bf16[8,4,512]{2,1,0:T(4,128)(2,1)} fusion(bf16[8,4,512]{2,1,0:T(4,128)(2,1)S(1)} %collective-permute-done.6, bf16[8,4,512]{2,1,0:T(4,128)(2,1)S(1)} %mix.1), kind=kLoop, calls=%fused_computation | loop fusion | flops 65536 | bytes 98304 | tf_op jit(solution)/shard_map/convert_element_type | solution.py:586
  (2 shorter events, 0.0 us)
Async XLA Ops:
  0.6 8.8 %copy-start = (f32[2,24,64,128]{3,2,1,0:T(8,128)S(1)}, f32[2,24,64,128]{3,2,1,0:T(8,128)}, u32[]{:S(2)}) copy-start(f32[2,24,64,128]{3,2,1,0:T(8,128)} %state.3) | copy-start | bytes 4718596
  0.7 8.8 %copy-start.2 = (bf16[2,7,1536]{2,0,1:T(2,128)(2,1)S(1)}, bf16[2,7,1536]{2,0,1:T(2,128)(2,1)}, u32[]{:S(2)}) copy-start(bf16[2,7,1536]{2,0,1:T(2,128)(2,1)} %param.39) | copy-start | bytes 129028
  0.7 8.8 %copy-start.3 = (bf16[2,7,2,512]{3,2,1,0:T(2,128)(2,1)S(1)}, bf16[2,7,2,512]{3,2,1,0:T(2,128)(2,1)}, u32[]{:S(2)}) copy-start(bf16[2,7,2,512]{3,2,1,0:T(2,128)(2,1)} %maps_window.1) | copy-start | bytes 86020
  0.7 8.8 %copy-start.4 = (bf16[2,4,1536]{2,1,0:T(4,128)(2,1)S(1)}, bf16[2,4,1536]{2,1,0:T(4,128)(2,1)}, u32[]{:S(2)}) copy-start(bf16[2,4,1536]{2,1,0:T(4,128)(2,1)} %past_x.1) | copy-start | bytes 73732
  0.7 8.8 %copy-start.5 = (bf16[4,3072]{1,0:T(4,128)(2,1)S(1)}, bf16[4,3072]{1,0:T(4,128)(2,1)}, u32[]{:S(2)}) copy-start(bf16[4,3072]{1,0:T(4,128)(2,1)} %head_taps.1) | copy-start | bytes 73732
  0.7 8.8 %copy-start.6 = (bf16[4,2,1024]{2,1,0:T(2,128)(2,1)S(1)}, bf16[4,2,1024]{2,1,0:T(2,128)(2,1)}, u32[]{:S(2)}) copy-start(bf16[4,2,1024]{2,1,0:T(2,128)(2,1)} %map_taps.1) | copy-start | bytes 49156
  0.7 8.8 %copy-start.7 = (bf16[2,4,512]{2,1,0:T(4,128)(2,1)S(1)}, bf16[2,4,512]{2,1,0:T(4,128)(2,1)}, u32[]{:S(2)}) copy-start(bf16[2,4,512]{2,1,0:T(4,128)(2,1)} %past_maps.1) | copy-start | bytes 24580
  0.7 8.8 %copy-start.8 = (bf16[3072]{0:T(1024)(128)(2,1)S(1)}, bf16[3072]{0:T(1024)(128)(2,1)}, u32[]{:S(2)}) copy-start(bf16[3072]{0:T(1024)(128)(2,1)} %param.33) | copy-start | bytes 18436
  0.7 8.8 %copy-start.9 = (f32[2,4,24]{2,1,0:T(4,128)S(1)}, f32[2,4,24]{2,1,0:T(4,128)}, u32[]{:S(2)}) copy-start(f32[2,4,24]{2,1,0:T(4,128)} %past_logs.1) | copy-start | bytes 2308
  0.7 8.8 %copy-start.11 = (s32[2]{0:T(128)S(1)}, s32[2]{0:T(128)}, u32[]{:S(2)}) copy-start(s32[2]{0:T(128)} %acc.1) | copy-start | bytes 28
  0.7 8.8 %copy-start.12 = (f32[48]{0:T(128)S(1)}, f32[48]{0:T(128)}, u32[]{:S(2)}) copy-start(f32[48]{0:T(128)} %param.27) | copy-start | bytes 580
  0.8 8.8 %copy-start.13 = (f32[48]{0:T(128)S(1)}, f32[48]{0:T(128)}, u32[]{:S(2)}) copy-start(f32[48]{0:T(128)} %param.28) | copy-start | bytes 580
  0.8 8.8 %copy-start.14 = (f32[48]{0:T(128)S(1)}, f32[48]{0:T(128)}, u32[]{:S(2)}) copy-start(f32[48]{0:T(128)} %param.32) | copy-start | bytes 580
  3.7 11.8 %copy-start.10 = (f32[2,4,24]{2,1,0:T(4,128)S(1)}, f32[2,4,24]{2,1,0:T(4,128)}, u32[]{:S(2)}) copy-start(f32[2,4,24]{2,1,0:T(4,128)} %decay_total.1) | copy-start | bytes 2308
  3.7 18.8 %copy-start.1 = (bf16[1536,512]{1,0:T(8,128)(2,1)S(1)}, bf16[1536,512]{1,0:T(8,128)(2,1)}, u32[]{:S(2)}) copy-start(bf16[1536,512]{1,0:T(8,128)(2,1)} %weight.1) | copy-start | bytes 4718596
  3.7 8.5 %collective-permute-start = (bf16[8,4224]{1,0:T(8,128)(2,1)S(1)}, bf16[8,4224]{1,0:T(8,128)(2,1)S(1)}, u32[]{:S(2)}, u32[]{:S(2)}) collective-permute-start(bf16[8,4224]{1,0:T(8,128)(2,1)S(1)} %get-tuple-element.35), channel_id=1, source_target_pairs={{0,4},{2,6},{4,0},{6,2},{1,5},{3,7},{5,1},{7,3},{8,12},{10,14},{12... | collective-permute-start | bytes 202760 | tf_op jit(solution)/shard_map/ppermute | solution.py:37
  7.8 4.4 %collective-permute-start.1 = (bf16[8,4224]{1,0:T(8,128)(2,1)S(1)}, bf16[8,4224]{1,0:T(8,128)(2,1)S(1)}, u32[]{:S(2)}, u32[]{:S(2)}) collective-permute-start(bf16[8,4224]{1,0:T(8,128)(2,1)S(1)} %get-tuple-element.36), channel_id=1, source_target_pairs={{0,2},{2,0},{4,6},{6,4},{1,3},{3,1},{5,7},{7,5},{8,10},{10,8},{12,... | collective-permute-start | bytes 202760 | tf_op jit(solution)/shard_map/ppermute | solution.py:37
  9.4 6.1 %collective-permute-start.2 = (bf16[8,4224]{1,0:T(8,128)(2,1)S(1)}, bf16[8,4224]{1,0:T(8,128)(2,1)S(1)}, u32[]{:S(2)}, u32[]{:S(2)}) collective-permute-start(bf16[8,4224]{1,0:T(8,128)(2,1)S(1)} %get-tuple-element.37), channel_id=1, source_target_pairs={{0,6},{2,4},{4,2},{6,0},{1,7},{3,5},{5,3},{7,1},{8,14},{10,12},{12... | collective-permute-start | bytes 202760 | tf_op jit(solution)/shard_map/ppermute | solution.py:37
  16.1 5.6 %collective-permute-start.5 = (bf16[8,1536]{1,0:T(8,128)(2,1)S(1)}, bf16[8,1536]{1,0:T(8,128)(2,1)S(1)}, u32[]{:S(2)}, u32[]{:S(2)}) collective-permute-start(bf16[8,1536]{1,0:T(8,128)(2,1)S(1)} %get-tuple-element.38.rest_0_), channel_id=1, source_target_pairs={{0,6},{2,4},{4,2},{6,0},{1,7},{3,5},{5,3},{7,1},{8,14},{10,12},{12... | collective-permute-start | bytes 73736 | tf_op jit(solution)/shard_map/ppermute | solution.py:37
  17.5 5.0 %collective-permute-start.4 = (bf16[8,1536]{1,0:T(8,128)(2,1)S(1)}, bf16[8,1536]{1,0:T(8,128)(2,1)S(1)}, u32[]{:S(2)}, u32[]{:S(2)}) collective-permute-start(bf16[8,1536]{1,0:T(8,128)(2,1)S(1)} %get-tuple-element.38.rest_0_), channel_id=1, source_target_pairs={{0,4},{2,6},{4,0},{6,2},{1,5},{3,7},{5,1},{7,3},{8,12},{10,14},{12... | collective-permute-start | bytes 73736 | tf_op jit(solution)/shard_map/ppermute | solution.py:37
  17.7 4.8 %collective-permute-start.3 = (bf16[8,1536]{1,0:T(8,128)(2,1)S(1)}, bf16[8,1536]{1,0:T(8,128)(2,1)S(1)}, u32[]{:S(2)}, u32[]{:S(2)}) collective-permute-start(bf16[8,1536]{1,0:T(8,128)(2,1)S(1)} %get-tuple-element.38.rest_0_), channel_id=1, source_target_pairs={{0,2},{2,0},{4,6},{6,4},{1,3},{3,1},{5,7},{7,5},{8,10},{10,8},{12,... | collective-permute-start | bytes 73736 | tf_op jit(solution)/shard_map/ppermute | solution.py:37
  22.8 1.2 %collective-permute-start.6 = (bf16[8,4,512]{2,1,0:T(4,128)(2,1)S(1)}, bf16[8,4,512]{2,1,0:T(4,128)(2,1)S(1)}, u32[]{:S(2)}, u32[]{:S(2)}) collective-permute-start(bf16[8,4,512]{2,1,0:T(4,128)(2,1)S(1)} %mix.1), channel_id=1, source_target_pairs={{0,1},{1,0},{2,3},{3,2},{4,5},{5,4},{6,7},{7,6},{8,9},{9,8},{10,11... | collective-permute-start | bytes 98312 | tf_op jit(solution)/shard_map/ppermute | solution.py:37

commit v3 on v2

--- a/solution.py
+++ b/solution.py
@@ -25,16 +25,17 @@
     return pltpu.CompilerParams(vmem_limit_bytes=mib << 20)
 
 
-def peer(me, k, n, back=False):
+def peer(me, k, n, ring, back=False):
     if n > DIRECT:
         return k
-    if n & (n - 1) == 0:
-        return me ^ k
-    return lax.rem(me + (n - k if back else k), n)
-
-
-def permute(array, axis, k, n):
-    return lax.ppermute(array, axis, [(i, int(peer(i, k, n))) for i in range(n)])
+    if ring or n & (n - 1):
+        at = me + (n - k if back else k)
+        return at % n if isinstance(me, int) else lax.rem(at, n)
+    return me ^ k
+
+
+def permute(array, axis, k, n, ring=False):
+    return lax.ppermute(array, axis, [(i, peer(i, k, n, ring)) for i in range(n)])
 
 
 def pick(rows, index, count, width):
@@ -97,7 +98,7 @@
         copy.wait()
     parts = []
     for k in range(n_kv):
-        start = peer(kv, k, n_kv) * own
+        start = peer(kv, k, n_kv, False) * own
         for s in range(own):
             parts.append(tok[start + s].astype(f32))
     values = jnp.concatenate(parts, axis=0)
@@ -401,7 +402,7 @@
         heads_window[keep + t] = jnp.concatenate(both, axis=0).astype(bf16)
 
 
-def mix_kernel(n_kv, weight, *rest):
+def mix_kernel(n_kv, order, weight, *rest):
     blocks, out = rest[:-1], rest[-1]
     kv = lax.axis_index("kv")
     _, props, _ = out.shape
@@ -412,10 +413,10 @@
     own = rows // props
     left = jnp.concatenate([piece.astype(f32) for piece in pieces], axis=0).astype(bf16)
     part = jnp.dot(left, weight[...], preferred_element_type=f32)
-    for k in range(n_kv):
-        start = peer(kv, k, n_kv, back=True) * own
+    for i, k in enumerate(order):
+        start = peer(kv, k, n_kv, True, back=True) * own
         for s in range(own):
-            at = k * rows + s * props
+            at = i * rows + s * props
             out[start + s] = part[at : at + props].astype(bf16)
 
 
@@ -495,7 +496,8 @@
         )
     )
     if n_kv <= DIRECT:
-        got = [permute(sent[k], "kv", k, n_kv) for k in (2, 1, 3)]
+        order = sorted(range(1, n_kv), key=lambda k: (k % 2, k))
+        got = [permute(sent[k], "kv", k, n_kv) for k in order]
         got = [sent[0]] + got
     else:
         got = [lax.all_to_all(jnp.stack(sent), "kv", 0, 0)]
@@ -555,10 +557,11 @@
     )(proposal_decay_total, state_low, conv_tail, taps, vectors, small, *got)
 
     if n_kv <= DIRECT:
-        gd = {k: permute(normed, "kv", k, n_kv) for k in (3, 2, 1)}
-        gathered = [normed] + [gd[k] for k in sorted(gd)]
+        order = (0, *reversed(range(1, n_kv)))
+        gathered = [normed] + [permute(normed, "kv", k, n_kv, True) for k in order[1:]]
     else:
         gathered = [lax.all_gather(normed, "kv")]
+        order = tuple(range(n_kv))
 
     head_input, input_maps, log_decays, heads_window, maps_window = pl.pallas_call(
         outputs_kernel,
@@ -574,7 +577,7 @@
     )(raw, weighted, maps, logs, tail_x, tail_maps)
 
     part = pl.pallas_call(
-        functools.partial(mix_kernel, n_kv),
+        functools.partial(mix_kernel, n_kv, order),
         out_shape=sds((seqs, props, local_d), bf16),
         compiler_params=params(8),
         name="mix",

time: 24.8 us -> 24.7 us (level)
  no operation moved by 1% of the time
where the time goes in v3:
time: 24.7 us; the launch traced here: 24.6 us
  starting transfers between devices  10.1 us (41%)
  Pallas kernels  7.22 us (29%)
  waiting for transfers between devices  5.63 us (23%)
  between operations  0.88 us (4%)
  other arithmetic  0.64 us (3%)
    ppermute x7, starting transfers between devices, permute(): lax.ppermute(array, axis, [(i, peer(i, k, n, ring)) for i in range(n)])  10.1 us
    ppermute x7, waiting for transfers between devices, permute(): lax.ppermute(array, axis, [(i, peer(i, k, n, ring)) for i in range(n)])  5.63 us
    pallas_call x1, Pallas kernels, local(): pl.pallas_call(functools.partial(project_kernel, n_kv, n_tp, chunk), out_...  2.9 us
    pallas_call x1, Pallas kernels, local(): pl.pallas_call(functools.partial(state_kernel, n_tp), out_shape=[sds(prio...  2.67 us
    pallas_call x1, Pallas kernels, local(): pl.pallas_call(outputs_kernel, out_shape=[sds((own, props, width), bf16),...  0.67 us
    convert_element_type x1, other arithmetic, local(): total.astype(bf16)  0.64 us
    pallas_call x1, Pallas kernels, local(): pl.pallas_call(functools.partial(mixer_kernel, local_d * n_kv, len(got)),...  0.62 us
  transfers between devices with their start and end apart: 7, of which 4 were waited for; matrix products, arithmetic and copies ran while one was open for 0% of the time, Pallas kernels for 14%

profile of v3, /device:TPU:0, one launch (start us, length us, event | category | flops | bytes accessed | tf_op | source)
XLA Modules:
  0.0 24.6 jit_solution(12186737660273513853)
XLA Ops:
  0.6 0.0 copy-start
  0.7 0.0 copy-start.2
  0.7 0.0 copy-start.3
  0.7 0.0 copy-start.4
  0.7 0.0 copy-start.5
  0.7 0.0 copy-start.6
  0.7 0.0 copy-start.7
  0.7 0.0 copy-start.8
  0.7 0.0 copy-start.9
  0.7 0.0 copy-start.11
  0.7 0.0 copy-start.12
  0.8 0.0 copy-start.13
  0.8 0.0 copy-start.14
  0.8 2.9 %project.1 = (bf16[8,4224]{1,0:T(8,128)(2,1)S(1)}, bf16[8,4224]{1,0:T(8,128)(2,1)S(1)}, bf16[8,4224]{1,0:T(8,128)(2,1)S(1)}, bf16[8,4224]{1,0:T(8,128)(2,1)S(1)}) custom-call(bf16[8,4,512]{2,1,0:T(4,128)(2,1)} %tok_hbm.1, bf16[16,128]{1,0:T(8,128)(2,1)} %bitcast.14, bf16[512,1536]{1,0:T(8,128)(2,1)} %wx.1, bf16[512,2,512]{2,1,0:T(2,128)(2,1)} %wm.1, ...), custom_call_target="tpu_custom_call" | custom-call | tf_op jit(solution)/shard_map/project/pallas_call | solution.py:469
  3.7 0.0 copy-start.10
  3.7 0.0 copy-start.1
  3.7 4.1 %collective-permute-start = (bf16[8,4224]{1,0:T(8,128)(2,1)S(1)}, bf16[8,4224]{1,0:T(8,128)(2,1)S(1)}, u32[]{:S(2)}, u32[]{:S(2)}) collective-permute-start(bf16[8,4224]{1,0:T(8,128)(2,1)S(1)} %get-tuple-element.35), channel_id=1, source_target_pairs={{0,4},{2,6},{4,0},{6,2},{1,5},{3,7},{5,1},{7,3},{8,12},{10,14},{12... | collective-permute-start | bytes 202760 | tf_op jit(solution)/shard_map/ppermute | solution.py:38
  7.8 1.6 %collective-permute-start.1 = (bf16[8,4224]{1,0:T(8,128)(2,1)S(1)}, bf16[8,4224]{1,0:T(8,128)(2,1)S(1)}, u32[]{:S(2)}, u32[]{:S(2)}) collective-permute-start(bf16[8,4224]{1,0:T(8,128)(2,1)S(1)} %get-tuple-element.36), channel_id=1, source_target_pairs={{0,2},{2,0},{4,6},{6,4},{1,3},{3,1},{5,7},{7,5},{8,10},{10,8},{12,... | collective-permute-start | bytes 202760 | tf_op jit(solution)/shard_map/ppermute | solution.py:38
  9.4 0.0 collective-permute-start.2
  9.4 0.0 copy-done
  9.4 0.0 copy-done.2
  9.4 0.0 copy-done.3
  9.4 0.0 copy-done.4
  9.4 0.0 copy-done.5
  9.5 0.0 copy-done.6
  9.5 0.0 copy-done.7
  9.5 0.0 copy-done.8
  9.5 0.0 copy-done.9
  9.5 0.0 copy-done.11
  9.5 0.0 copy-done.12
  9.5 0.0 copy-done.13
  9.5 0.0 copy-done.14
  9.5 2.7 %state.2 = (f32[2,24,64,128]{3,2,1,0:T(8,128)}, bf16[2,1536,128]{2,1,0:T(8,128)(2,1)S(1)}, bf16[3,2,1536]{2,1,0:T(2,128)(2,1)S(1)}, bf16[2,3,2,512]{3,2,1,0:T(2,...) custom-call(s32[2]{0:T(128)S(1)} %copy-done.11, ...), custom_call_target="tpu_custom_call" | custom-call | tf_op jit(solution)/shard_map/state/pallas_call | solution.py:514
  12.2 0.0 collective-permute-done.rest_1_
  12.2 0.0 collective-permute-done.1.rest_2_
  12.2 3.3 %collective-permute-done.2.rest_3_ = bf16[8,4224]{1,0:T(8,128)(2,1)S(1)} collective-permute-done((bf16[8,4224]{1,0:T(8,128)(2,1)S(1)}, bf16[8,4224]{1,0:T(8,128)(2,1)S(1)}, u32[]{:S(2)}, u32[]{:S(2)}) %collective-permute-start.2) | collective-permute-done | bytes 67616 | tf_op jit(solution)/shard_map/ppermute | solution.py:38
  15.5 0.6 %mixer.1 = (bf16[8,1536]{1,0:T(8,128)(2,1)S(1)}, bf16[8,2560]{1,0:T(8,128)(2,1)S(1)}, f32[8,1536]{1,0:T(8,128)S(1)}, f32[8,512]{1,0:T(8,128)S(1)}, f32[8,24]{1,0:T(8,128)S(1)}) custom-call(f32[2,4,24]{2,1,0:T(4,128)S(1)} %copy-done.10, bf16[2,1536,128]{2,1,0:T(8,128)(2,1)S(1)} %get-tuple-element.29.state_low, f32[8,2560]{1,0:T(8,128)S(1)} %get-tuple-element.30.conv_tail, ...), custom_call_target="tpu_custom_call" | custom-call | tf_op jit(solution)/shard_map/mixer/pallas_call | solution.py:546
  16.1 0.0 collective-permute-start.5
  16.1 1.9 %collective-permute-start.4 = (bf16[8,1536]{1,0:T(8,128)(2,1)S(1)}, bf16[8,1536]{1,0:T(8,128)(2,1)S(1)}, u32[]{:S(2)}, u32[]{:S(2)}) collective-permute-start(bf16[8,1536]{1,0:T(8,128)(2,1)S(1)} %get-tuple-element.38.rest_0_), channel_id=1, source_target_pairs={{0,4},{2,6},{4,0},{6,2},{1,5},{3,7},{5,1},{7,3},{8,12},{10,14},{12... | collective-permute-start | bytes 73736 | tf_op jit(solution)/shard_map/ppermute | solution.py:38
  18.0 2.5 %collective-permute-start.3 = (bf16[8,1536]{1,0:T(8,128)(2,1)S(1)}, bf16[8,1536]{1,0:T(8,128)(2,1)S(1)}, u32[]{:S(2)}, u32[]{:S(2)}) collective-permute-start(bf16[8,1536]{1,0:T(8,128)(2,1)S(1)} %get-tuple-element.38.rest_0_), channel_id=1, source_target_pairs={{0,6},{2,0},{4,2},{6,4},{1,7},{3,1},{5,3},{7,5},{8,14},{10,8},{12,... | collective-permute-start | bytes 73736 | tf_op jit(solution)/shard_map/ppermute | solution.py:38
  20.5 1.2 %collective-permute-done.5.rest_3_ = bf16[8,1536]{1,0:T(8,128)(2,1)S(1)} collective-permute-done((bf16[8,1536]{1,0:T(8,128)(2,1)S(1)}, bf16[8,1536]{1,0:T(8,128)(2,1)S(1)}, u32[]{:S(2)}, u32[]{:S(2)}) %collective-permute-start.5) | collective-permute-done | bytes 24608 | tf_op jit(solution)/shard_map/ppermute | solution.py:38
  21.8 0.0 collective-permute-done.4.rest_2_
  21.8 0.6 %collective-permute-done.3.rest_1_ = bf16[8,1536]{1,0:T(8,128)(2,1)S(1)} collective-permute-done((bf16[8,1536]{1,0:T(8,128)(2,1)S(1)}, bf16[8,1536]{1,0:T(8,128)(2,1)S(1)}, u32[]{:S(2)}, u32[]{:S(2)}) %collective-permute-start.3) | collective-permute-done | bytes 24608 | tf_op jit(solution)/shard_map/ppermute | solution.py:38
  22.3 0.4 %mix.1 = bf16[8,4,512]{2,1,0:T(4,128)(2,1)S(1)} custom-call(bf16[1536,512]{1,0:T(8,128)(2,1)S(1)} %copy-done.1, bf16[8,1536]{1,0:T(8,128)(2,1)S(1)} %get-tuple-element.38.rest_0_, bf16[8,1536]{1,0:T(8,128)(2,1)S(1)} %collective-permute-done.3.rest_1_, bf16[8,1536]{1,0:T(8,128)(2,1)S(1)} %collective-permute-done.4.rest_2_, ...), custom_call_target="tpu_custom_call" | custom-call | tf_op jit(solution)/shard_map/mix/pallas_call | solution.py:579
  22.7 0.0 collective-permute-start.6
  22.7 0.7 %outputs.1 = (bf16[2,4,1536]{2,1,0:T(4,128)(2,1)}, bf16[2,4,512]{2,1,0:T(4,128)(2,1)}, f32[2,4,24]{2,1,0:T(4,128)}, bf16[7,2,1536]{2,1,0:T(2,128)(2,1)}, bf16[2,7,2,512]{3,2,1,0:T(2,128)(2,1)}) custom-call(bf16[8,2560]{1,0:T(8,128)(2,1)S(1)} %get-tuple-element.40.raw, f32[8,1536]{1,0:T(8,128)S(1)} %get-tuple-element.41.weighted, ...), custom_call_target="tpu_custom_call" | custom-call | tf_op jit(solution)/shard_map/outputs/pallas_call | solution.py:566
  23.4 0.5 %collective-permute-done.6 = bf16[8,4,512]{2,1,0:T(4,128)(2,1)S(1)} collective-permute-done((bf16[8,4,512]{2,1,0:T(4,128)(2,1)S(1)}, bf16[8,4,512]{2,1,0:T(4,128)(2,1)S(1)}, u32[]{:S(2)}, u32[]{:S(2)}) %collective-permute-start.6) | collective-permute-done | bytes 32800 | tf_op jit(solution)/shard_map/ppermute | solution.py:38
  23.9 0.6 %add_convert_fusion = bf16[8,4,512]{2,1,0:T(4,128)(2,1)} fusion(bf16[8,4,512]{2,1,0:T(4,128)(2,1)S(1)} %collective-permute-done.6, bf16[8,4,512]{2,1,0:T(4,128)(2,1)S(1)} %mix.1), kind=kLoop, calls=%fused_computation | loop fusion | flops 65536 | bytes 98304 | tf_op jit(solution)/shard_map/convert_element_type | solution.py:589
  (2 shorter events, 0.0 us)
Async XLA Ops:
  0.6 8.8 %copy-start = (f32[2,24,64,128]{3,2,1,0:T(8,128)S(1)}, f32[2,24,64,128]{3,2,1,0:T(8,128)}, u32[]{:S(2)}) copy-start(f32[2,24,64,128]{3,2,1,0:T(8,128)} %state.3) | copy-start | bytes 4718596
  0.7 8.8 %copy-start.2 = (bf16[2,7,1536]{2,0,1:T(2,128)(2,1)S(1)}, bf16[2,7,1536]{2,0,1:T(2,128)(2,1)}, u32[]{:S(2)}) copy-start(bf16[2,7,1536]{2,0,1:T(2,128)(2,1)} %param.39) | copy-start | bytes 129028
  0.7 8.8 %copy-start.3 = (bf16[2,7,2,512]{3,2,1,0:T(2,128)(2,1)S(1)}, bf16[2,7,2,512]{3,2,1,0:T(2,128)(2,1)}, u32[]{:S(2)}) copy-start(bf16[2,7,2,512]{3,2,1,0:T(2,128)(2,1)} %maps_window.1) | copy-start | bytes 86020
  0.7 8.8 %copy-start.4 = (bf16[2,4,1536]{2,1,0:T(4,128)(2,1)S(1)}, bf16[2,4,1536]{2,1,0:T(4,128)(2,1)}, u32[]{:S(2)}) copy-start(bf16[2,4,1536]{2,1,0:T(4,128)(2,1)} %past_x.1) | copy-start | bytes 73732
  0.7 8.8 %copy-start.5 = (bf16[4,3072]{1,0:T(4,128)(2,1)S(1)}, bf16[4,3072]{1,0:T(4,128)(2,1)}, u32[]{:S(2)}) copy-start(bf16[4,3072]{1,0:T(4,128)(2,1)} %head_taps.1) | copy-start | bytes 73732
  0.7 8.8 %copy-start.6 = (bf16[4,2,1024]{2,1,0:T(2,128)(2,1)S(1)}, bf16[4,2,1024]{2,1,0:T(2,128)(2,1)}, u32[]{:S(2)}) copy-start(bf16[4,2,1024]{2,1,0:T(2,128)(2,1)} %map_taps.1) | copy-start | bytes 49156
  0.7 8.8 %copy-start.7 = (bf16[2,4,512]{2,1,0:T(4,128)(2,1)S(1)}, bf16[2,4,512]{2,1,0:T(4,128)(2,1)}, u32[]{:S(2)}) copy-start(bf16[2,4,512]{2,1,0:T(4,128)(2,1)} %past_maps.1) | copy-start | bytes 24580
  0.7 8.8 %copy-start.8 = (bf16[3072]{0:T(1024)(128)(2,1)S(1)}, bf16[3072]{0:T(1024)(128)(2,1)}, u32[]{:S(2)}) copy-start(bf16[3072]{0:T(1024)(128)(2,1)} %param.33) | copy-start | bytes 18436
  0.7 8.8 %copy-start.9 = (f32[2,4,24]{2,1,0:T(4,128)S(1)}, f32[2,4,24]{2,1,0:T(4,128)}, u32[]{:S(2)}) copy-start(f32[2,4,24]{2,1,0:T(4,128)} %past_logs.1) | copy-start | bytes 2308
  0.7 8.8 %copy-start.11 = (s32[2]{0:T(128)S(1)}, s32[2]{0:T(128)}, u32[]{:S(2)}) copy-start(s32[2]{0:T(128)} %acc.1) | copy-start | bytes 28
  0.7 8.8 %copy-start.12 = (f32[48]{0:T(128)S(1)}, f32[48]{0:T(128)}, u32[]{:S(2)}) copy-start(f32[48]{0:T(128)} %param.27) | copy-start | bytes 580
  0.8 8.8 %copy-start.13 = (f32[48]{0:T(128)S(1)}, f32[48]{0:T(128)}, u32[]{:S(2)}) copy-start(f32[48]{0:T(128)} %param.28) | copy-start | bytes 580
  0.8 8.8 %copy-start.14 = (f32[48]{0:T(128)S(1)}, f32[48]{0:T(128)}, u32[]{:S(2)}) copy-start(f32[48]{0:T(128)} %param.32) | copy-start | bytes 580
  3.7 11.8 %copy-start.10 = (f32[2,4,24]{2,1,0:T(4,128)S(1)}, f32[2,4,24]{2,1,0:T(4,128)}, u32[]{:S(2)}) copy-start(f32[2,4,24]{2,1,0:T(4,128)} %decay_total.1) | copy-start | bytes 2308
  3.7 18.6 %copy-start.1 = (bf16[1536,512]{1,0:T(8,128)(2,1)S(1)}, bf16[1536,512]{1,0:T(8,128)(2,1)}, u32[]{:S(2)}) copy-start(bf16[1536,512]{1,0:T(8,128)(2,1)} %weight.1) | copy-start | bytes 4718596
  3.7 8.5 %collective-permute-start = (bf16[8,4224]{1,0:T(8,128)(2,1)S(1)}, bf16[8,4224]{1,0:T(8,128)(2,1)S(1)}, u32[]{:S(2)}, u32[]{:S(2)}) collective-permute-start(bf16[8,4224]{1,0:T(8,128)(2,1)S(1)} %get-tuple-element.35), channel_id=1, source_target_pairs={{0,4},{2,6},{4,0},{6,2},{1,5},{3,7},{5,1},{7,3},{8,12},{10,14},{12... | collective-permute-start | bytes 202760 | tf_op jit(solution)/shard_map/ppermute | solution.py:38
  7.8 4.4 %collective-permute-start.1 = (bf16[8,4224]{1,0:T(8,128)(2,1)S(1)}, bf16[8,4224]{1,0:T(8,128)(2,1)S(1)}, u32[]{:S(2)}, u32[]{:S(2)}) collective-permute-start(bf16[8,4224]{1,0:T(8,128)(2,1)S(1)} %get-tuple-element.36), channel_id=1, source_target_pairs={{0,2},{2,0},{4,6},{6,4},{1,3},{3,1},{5,7},{7,5},{8,10},{10,8},{12,... | collective-permute-start | bytes 202760 | tf_op jit(solution)/shard_map/ppermute | solution.py:38
  9.4 6.1 %collective-permute-start.2 = (bf16[8,4224]{1,0:T(8,128)(2,1)S(1)}, bf16[8,4224]{1,0:T(8,128)(2,1)S(1)}, u32[]{:S(2)}, u32[]{:S(2)}) collective-permute-start(bf16[8,4224]{1,0:T(8,128)(2,1)S(1)} %get-tuple-element.37), channel_id=1, source_target_pairs={{0,6},{2,4},{4,2},{6,0},{1,7},{3,5},{5,3},{7,1},{8,14},{10,12},{12... | collective-permute-start | bytes 202760 | tf_op jit(solution)/shard_map/ppermute | solution.py:38
  16.1 5.6 %collective-permute-start.5 = (bf16[8,1536]{1,0:T(8,128)(2,1)S(1)}, bf16[8,1536]{1,0:T(8,128)(2,1)S(1)}, u32[]{:S(2)}, u32[]{:S(2)}) collective-permute-start(bf16[8,1536]{1,0:T(8,128)(2,1)S(1)} %get-tuple-element.38.rest_0_), channel_id=1, source_target_pairs={{0,2},{2,4},{4,6},{6,0},{1,3},{3,5},{5,7},{7,1},{8,10},{10,12},{12... | collective-permute-start | bytes 73736 | tf_op jit(solution)/shard_map/ppermute | solution.py:38
  16.1 5.6 %collective-permute-start.4 = (bf16[8,1536]{1,0:T(8,128)(2,1)S(1)}, bf16[8,1536]{1,0:T(8,128)(2,1)S(1)}, u32[]{:S(2)}, u32[]{:S(2)}) collective-permute-start(bf16[8,1536]{1,0:T(8,128)(2,1)S(1)} %get-tuple-element.38.rest_0_), channel_id=1, source_target_pairs={{0,4},{2,6},{4,0},{6,2},{1,5},{3,7},{5,1},{7,3},{8,12},{10,14},{12... | collective-permute-start | bytes 73736 | tf_op jit(solution)/shard_map/ppermute | solution.py:38
  18.0 4.3 %collective-permute-start.3 = (bf16[8,1536]{1,0:T(8,128)(2,1)S(1)}, bf16[8,1536]{1,0:T(8,128)(2,1)S(1)}, u32[]{:S(2)}, u32[]{:S(2)}) collective-permute-start(bf16[8,1536]{1,0:T(8,128)(2,1)S(1)} %get-tuple-element.38.rest_0_), channel_id=1, source_target_pairs={{0,6},{2,0},{4,2},{6,4},{1,7},{3,1},{5,3},{7,5},{8,14},{10,8},{12,... | collective-permute-start | bytes 73736 | tf_op jit(solution)/shard_map/ppermute | solution.py:38
  22.7 1.2 %collective-permute-start.6 = (bf16[8,4,512]{2,1,0:T(4,128)(2,1)S(1)}, bf16[8,4,512]{2,1,0:T(4,128)(2,1)S(1)}, u32[]{:S(2)}, u32[]{:S(2)}) collective-permute-start(bf16[8,4,512]{2,1,0:T(4,128)(2,1)S(1)} %mix.1), channel_id=1, source_target_pairs={{0,1},{1,0},{2,3},{3,2},{4,5},{5,4},{6,7},{7,6},{8,9},{9,8},{10,11... | collective-permute-start | bytes 98312 | tf_op jit(solution)/shard_map/ppermute | solution.py:38

commit v4 on v3

--- a/solution.py
+++ b/solution.py
@@ -163,6 +163,8 @@
 
 def state_kernel(
     n_tp,
+    arrive,
+    leave,
     acc,
     state,
     past_x,
@@ -176,7 +178,6 @@
     speed,
     direct,
     norm_gain,
-    new_state,
     state_low,
     tail_x,
     tail_maps,
@@ -248,6 +249,7 @@
             coefficients[j] = jnp.where(j < a, jnp.exp(after), 0.0)
             after = after + jnp.where(j < a, logs[j : j + 1], 0.0)
         factor = jnp.exp(after)
+        arrive(s)
         coefficient = spread(jnp.concatenate(coefficients, axis=0), heads)
         scaled = past_x[s].astype(f32) * coefficient
         high = scaled.astype(bf16).astype(f32)
@@ -266,8 +268,43 @@
                 h = g * per_group + i
                 value = state[s, h] * factor[:, h : h + 1]
                 value = value + update[i * HEAD_DIM : (i + 1) * HEAD_DIM]
-                new_state[s, h] = value
+                state[s, h] = value
                 state_low[s, h * HEAD_DIM : (h + 1) * HEAD_DIM, :] = value.astype(bf16)
+        leave(s)
+
+
+def fetched_state_kernel(n_tp, acc, state_hbm, *rest):
+    sources, new_state, outs, rest = rest[:11], rest[11], rest[12:19], rest[19:]
+    gain_rows, state, targets, sems, state_sems = rest[0], rest[1], rest[2:13], rest[13], rest[14]
+    own = state.shape[0]
+    small = [
+        pltpu.make_async_copy(source, target, sems.at[i])
+        for i, (source, target) in enumerate(zip(sources, targets, strict=True))
+    ]
+    inward = [
+        pltpu.make_async_copy(state_hbm.at[s], state.at[s], state_sems.at[0, s])
+        for s in range(own)
+    ]
+    outward = [
+        pltpu.make_async_copy(state.at[s], new_state.at[s], state_sems.at[1, s])
+        for s in range(own)
+    ]
+    for copy in small + inward:
+        copy.start()
+    for copy in small:
+        copy.wait()
+    state_kernel(
+        n_tp,
+        lambda s: inward[s].wait(),
+        lambda s: outward[s].start(),
+        acc,
+        state,
+        *targets,
+        *outs,
+        gain_rows,
+    )
+    for copy in outward:
+        copy.wait()
 
 
 def mixer_kernel(
@@ -496,39 +533,13 @@
         )
     )
     if n_kv <= DIRECT:
-        order = sorted(range(1, n_kv), key=lambda k: (k % 2, k))
+        order = [*range(2, n_kv), *range(1, min(2, n_kv))]
         got = [permute(sent[k], "kv", k, n_kv) for k in order]
         got = [sent[0]] + got
     else:
         got = [lax.all_to_all(jnp.stack(sent), "kv", 0, 0)]
 
-    (
-        accepted_state,
-        state_low,
-        tail_x,
-        tail_maps,
-        conv_tail,
-        taps,
-        vectors,
-        small,
-    ) = pl.pallas_call(
-        functools.partial(state_kernel, n_tp),
-        out_shape=[
-            sds(prior_state_value.shape, f32),
-            sds((own, width, STATE), bf16),
-            sds((CONV - 1, own, width), bf16),
-            sds((own, CONV - 1, 2, bc), bf16),
-            sds((rows, conv_width), f32),
-            sds((CONV, conv_width), f32),
-            sds((2, width), f32),
-            sds((2, LANES), f32),
-        ],
-        in_specs=[pl.BlockSpec(memory_space=pltpu.SMEM)] + [vmem] * 12,
-        scratch_shapes=[pltpu.VMEM((n_tp * width // LANES, LANES), f32)],
-        compiler_params=params(12),
-        name="state",
-    )(
-        accepted,
+    later = (
         prior_state_value,
         previous_head_input,
         previous_input_maps,
@@ -542,6 +553,38 @@
         head_direct_gain.reshape(1, -1),
         grouped_norm_gain.reshape(-1, LANES),
     )
+    (
+        accepted_state,
+        state_low,
+        tail_x,
+        tail_maps,
+        conv_tail,
+        taps,
+        vectors,
+        small,
+    ) = pl.pallas_call(
+        functools.partial(fetched_state_kernel, n_tp),
+        out_shape=[
+            sds(prior_state_value.shape, f32),
+            sds((own, width, STATE), bf16),
+            sds((CONV - 1, own, width), bf16),
+            sds((own, CONV - 1, 2, bc), bf16),
+            sds((rows, conv_width), f32),
+            sds((CONV, conv_width), f32),
+            sds((2, width), f32),
+            sds((2, LANES), f32),
+        ],
+        in_specs=[pl.BlockSpec(memory_space=pltpu.SMEM)] + [hbm] * 12,
+        scratch_shapes=[
+            pltpu.VMEM((n_tp * width // LANES, LANES), f32),
+            *(pltpu.VMEM(array.shape, array.dtype) for array in later),
+            pltpu.SemaphoreType.DMA((len(later) - 1,)),
+            pltpu.SemaphoreType.DMA((2, own)),
+        ],
+        out_specs=[hbm] + [vmem] * 7,
+        compiler_params=params(12),
+        name="state",
+    )(accepted, *(pltpu.with_memory_space_constraint(array, pltpu.HBM) for array in later))
 
     normed, raw, weighted, maps, logs = pl.pallas_call(
         functools.partial(mixer_kernel, local_d * n_kv, len(got)),

time: 24.7 us -> 24.5 us (level)
  waiting for transfers between devices: 5.63 us -> 3.22 us
  starting transfers between devices: 10.1 us -> 11.5 us
  Pallas kernels: 7.22 us -> 8.3 us
    ppermute x7, waiting for transfers between devices: 5.63 us -> 3.22 us  [permute(): lax.ppermute(array, axis, [(i, peer(i, k, n, ring)) for i in range(n)])]
    ppermute x7, starting transfers between devices: 10.1 us -> 11.5 us  [permute(): lax.ppermute(array, axis, [(i, peer(i, k, n, ring)) for i in range(n)])]
    pallas_call x1, Pallas kernels: 2.67 us -> 3.83 us  [local(): pl.pallas_call(functools.partial(fetched_state_kernel, n_tp), out_shape=[...]
  transfers between devices with their start and end apart: 7 -> 7, of which waited for: 4 -> 5; matrix products, arithmetic and copies ran while one was open for 0% -> 0% of each run, Pallas kernels for 14% -> 19%
where the time goes in v4:
time: 24.5 us; the launch traced here: 24.3 us
  starting transfers between devices  11.5 us (47%)
  Pallas kernels  8.3 us (34%)
  waiting for transfers between devices  3.22 us (13%)
  between operations  0.7 us (3%)
  other arithmetic  0.64 us (3%)
    ppermute x7, starting transfers between devices, permute(): lax.ppermute(array, axis, [(i, peer(i, k, n, ring)) for i in range(n)])  11.5 us
    pallas_call x1, Pallas kernels, local(): pl.pallas_call(functools.partial(fetched_state_kernel, n_tp), out_shape=[...  3.83 us
    ppermute x7, waiting for transfers between devices, permute(): lax.ppermute(array, axis, [(i, peer(i, k, n, ring)) for i in range(n)])  3.22 us
    pallas_call x1, Pallas kernels, local(): pl.pallas_call(functools.partial(project_kernel, n_kv, n_tp, chunk), out_...  2.82 us
    pallas_call x1, Pallas kernels, local(): pl.pallas_call(outputs_kernel, out_shape=[sds((own, props, width), bf16),...  0.67 us
    convert_element_type x1, other arithmetic, local(): total.astype(bf16)  0.64 us
    pallas_call x1, Pallas kernels, local(): pl.pallas_call(functools.partial(mixer_kernel, local_d * n_kv, len(got)),...  0.62 us
  transfers between devices with their start and end apart: 7, of which 5 were waited for; matrix products, arithmetic and copies ran while one was open for 0% of the time, Pallas kernels for 19%

profile of v4, /device:TPU:0, one launch (start us, length us, event | category | flops | bytes accessed | tf_op | source)
XLA Modules:
  0.0 24.3 jit_solution(15088818708070127926)
XLA Ops:
  0.6 0.0 copy-start.2
  0.6 2.8 %project.1 = (bf16[8,4224]{1,0:T(8,128)(2,1)S(1)}, bf16[8,4224]{1,0:T(8,128)(2,1)S(1)}, bf16[8,4224]{1,0:T(8,128)(2,1)S(1)}, bf16[8,4224]{1,0:T(8,128)(2,1)S(1)}) custom-call(bf16[8,4,512]{2,1,0:T(4,128)(2,1)} %tok_hbm.1, bf16[16,128]{1,0:T(8,128)(2,1)} %bitcast.11, bf16[512,1536]{1,0:T(8,128)(2,1)} %wx.1, bf16[512,2,512]{2,1,0:T(2,128)(2,1)} %wm.1, ...), custom_call_target="tpu_custom_call" | custom-call | tf_op jit(solution)/shard_map/project/pallas_call | solution.py:506
  3.5 0.0 copy-start.1
  3.5 0.0 copy-start
  3.5 4.1 %collective-permute-start = (bf16[8,4224]{1,0:T(8,128)(2,1)S(1)}, bf16[8,4224]{1,0:T(8,128)(2,1)S(1)}, u32[]{:S(2)}, u32[]{:S(2)}) collective-permute-start(bf16[8,4224]{1,0:T(8,128)(2,1)S(1)} %get-tuple-element.35), channel_id=1, source_target_pairs={{0,4},{2,6},{4,0},{6,2},{1,5},{3,7},{5,1},{7,3},{8,12},{10,14},{12... | collective-permute-start | bytes 202760 | tf_op jit(solution)/shard_map/ppermute | solution.py:38
  7.6 1.3 %collective-permute-start.1 = (bf16[8,4224]{1,0:T(8,128)(2,1)S(1)}, bf16[8,4224]{1,0:T(8,128)(2,1)S(1)}, u32[]{:S(2)}, u32[]{:S(2)}) collective-permute-start(bf16[8,4224]{1,0:T(8,128)(2,1)S(1)} %get-tuple-element.36), channel_id=1, source_target_pairs={{0,6},{2,4},{4,2},{6,0},{1,7},{3,5},{5,3},{7,1},{8,14},{10,12},{12... | collective-permute-start | bytes 202760 | tf_op jit(solution)/shard_map/ppermute | solution.py:38
  9.0 0.2 collective-permute-start.2
  9.2 0.0 copy-done.2
  9.2 3.8 %state.1 = (f32[2,24,64,128]{3,2,1,0:T(8,128)}, bf16[2,1536,128]{2,1,0:T(8,128)(2,1)S(1)}, bf16[3,2,1536]{2,1,0:T(2,128)(2,1)S(1)}, bf16[2,3,2,512]{3,2,1,0:T(2,...) custom-call(s32[2]{0:T(128)S(1)} %copy-done.2, ...), custom_call_target="tpu_custom_call" | custom-call | tf_op jit(solution)/shard_map/state/pallas_call | solution.py:565
  13.1 0.0 collective-permute-done.rest_1_
  13.1 0.8 %collective-permute-done.1.rest_2_ = bf16[8,4224]{1,0:T(8,128)(2,1)S(1)} collective-permute-done((bf16[8,4224]{1,0:T(8,128)(2,1)S(1)}, bf16[8,4224]{1,0:T(8,128)(2,1)S(1)}, u32[]{:S(2)}, u32[]{:S(2)}) %collective-permute-start.1) | collective-permute-done | bytes 67616 | tf_op jit(solution)/shard_map/ppermute | solution.py:38
  13.9 0.1 collective-permute-done.2.rest_3_
  14.0 0.0 copy-done.1
  14.0 0.6 %mixer.1 = (bf16[8,1536]{1,0:T(8,128)(2,1)S(1)}, bf16[8,2560]{1,0:T(8,128)(2,1)S(1)}, f32[8,1536]{1,0:T(8,128)S(1)}, f32[8,512]{1,0:T(8,128)S(1)}, f32[8,24]{1,0:T(8,128)S(1)}) custom-call(f32[2,4,24]{2,1,0:T(4,128)S(1)} %copy-done.1, bf16[2,1536,128]{2,1,0:T(8,128)(2,1)S(1)} %get-tuple-element.29.state_low, f32[8,2560]{1,0:T(8,128)S(1)} %get-tuple-element.30.conv_tail, ...), custom_call_target="tpu_custom_call" | custom-call | tf_op jit(solution)/shard_map/mixer/pallas_call | solution.py:589
  14.6 0.9 %collective-permute-start.5 = (bf16[8,1536]{1,0:T(8,128)(2,1)S(1)}, bf16[8,1536]{1,0:T(8,128)(2,1)S(1)}, u32[]{:S(2)}, u32[]{:S(2)}) collective-permute-start(bf16[8,1536]{1,0:T(8,128)(2,1)S(1)} %get-tuple-element.38.rest_0_), channel_id=1, source_target_pairs={{0,2},{2,4},{4,6},{6,0},{1,3},{3,5},{5,7},{7,1},{8,10},{10,12},{12... | collective-permute-start | bytes 73736 | tf_op jit(solution)/shard_map/ppermute | solution.py:38
  15.5 2.8 %collective-permute-start.4 = (bf16[8,1536]{1,0:T(8,128)(2,1)S(1)}, bf16[8,1536]{1,0:T(8,128)(2,1)S(1)}, u32[]{:S(2)}, u32[]{:S(2)}) collective-permute-start(bf16[8,1536]{1,0:T(8,128)(2,1)S(1)} %get-tuple-element.38.rest_0_), channel_id=1, source_target_pairs={{0,4},{2,6},{4,0},{6,2},{1,5},{3,7},{5,1},{7,3},{8,12},{10,14},{12... | collective-permute-start | bytes 73736 | tf_op jit(solution)/shard_map/ppermute | solution.py:38
  18.3 2.1 %collective-permute-start.3 = (bf16[8,1536]{1,0:T(8,128)(2,1)S(1)}, bf16[8,1536]{1,0:T(8,128)(2,1)S(1)}, u32[]{:S(2)}, u32[]{:S(2)}) collective-permute-start(bf16[8,1536]{1,0:T(8,128)(2,1)S(1)} %get-tuple-element.38.rest_0_), channel_id=1, source_target_pairs={{0,6},{2,0},{4,2},{6,4},{1,7},{3,1},{5,3},{7,5},{8,14},{10,8},{12,... | collective-permute-start | bytes 73736 | tf_op jit(solution)/shard_map/ppermute | solution.py:38
  20.4 0.0 collective-permute-done.5.rest_3_
  20.4 0.4 %collective-permute-done.4.rest_2_ = bf16[8,1536]{1,0:T(8,128)(2,1)S(1)} collective-permute-done((bf16[8,1536]{1,0:T(8,128)(2,1)S(1)}, bf16[8,1536]{1,0:T(8,128)(2,1)S(1)}, u32[]{:S(2)}, u32[]{:S(2)}) %collective-permute-start.4) | collective-permute-done | bytes 24608 | tf_op jit(solution)/shard_map/ppermute | solution.py:38
  20.8 1.3 %collective-permute-done.3.rest_1_ = bf16[8,1536]{1,0:T(8,128)(2,1)S(1)} collective-permute-done((bf16[8,1536]{1,0:T(8,128)(2,1)S(1)}, bf16[8,1536]{1,0:T(8,128)(2,1)S(1)}, u32[]{:S(2)}, u32[]{:S(2)}) %collective-permute-start.3) | collective-permute-done | bytes 24608 | tf_op jit(solution)/shard_map/ppermute | solution.py:38
  22.1 0.0 copy-done
  22.1 0.4 %mix.1 = bf16[8,4,512]{2,1,0:T(4,128)(2,1)S(1)} custom-call(bf16[1536,512]{1,0:T(8,128)(2,1)S(1)} %copy-done, bf16[8,1536]{1,0:T(8,128)(2,1)S(1)} %get-tuple-element.38.rest_0_, bf16[8,1536]{1,0:T(8,128)(2,1)S(1)} %collective-permute-done.3.rest_1_, bf16[8,1536]{1,0:T(8,128)(2,1)S(1)} %collective-permute-done.4.rest_2_, ...), custom_call_target="tpu_custom_call" | custom-call | tf_op jit(solution)/shard_map/mix/pallas_call | solution.py:622
  22.5 0.0 collective-permute-start.6
  22.5 0.7 %outputs.1 = (bf16[2,4,1536]{2,1,0:T(4,128)(2,1)}, bf16[2,4,512]{2,1,0:T(4,128)(2,1)}, f32[2,4,24]{2,1,0:T(4,128)}, bf16[7,2,1536]{2,1,0:T(2,128)(2,1)}, bf16[2,7,2,512]{3,2,1,0:T(2,128)(2,1)}) custom-call(bf16[8,2560]{1,0:T(8,128)(2,1)S(1)} %get-tuple-element.40.raw, f32[8,1536]{1,0:T(8,128)S(1)} %get-tuple-element.41.weighted, ...), custom_call_target="tpu_custom_call" | custom-call | tf_op jit(solution)/shard_map/outputs/pallas_call | solution.py:609
  23.2 0.5 %collective-permute-done.6 = bf16[8,4,512]{2,1,0:T(4,128)(2,1)S(1)} collective-permute-done((bf16[8,4,512]{2,1,0:T(4,128)(2,1)S(1)}, bf16[8,4,512]{2,1,0:T(4,128)(2,1)S(1)}, u32[]{:S(2)}, u32[]{:S(2)}) %collective-permute-start.6) | collective-permute-done | bytes 32800 | tf_op jit(solution)/shard_map/ppermute | solution.py:38
  23.7 0.6 %add_convert_fusion = bf16[8,4,512]{2,1,0:T(4,128)(2,1)} fusion(bf16[8,4,512]{2,1,0:T(4,128)(2,1)S(1)} %collective-permute-done.6, bf16[8,4,512]{2,1,0:T(4,128)(2,1)S(1)} %mix.1), kind=kLoop, calls=%fused_computation | loop fusion | flops 65536 | bytes 98304 | tf_op jit(solution)/shard_map/convert_element_type | solution.py:632
Async XLA Ops:
  0.6 8.6 %copy-start.2 = (s32[2]{0:T(128)S(1)}, s32[2]{0:T(128)}, u32[]{:S(2)}) copy-start(s32[2]{0:T(128)} %acc.1) | copy-start | bytes 28
  3.5 10.5 %copy-start.1 = (f32[2,4,24]{2,1,0:T(4,128)S(1)}, f32[2,4,24]{2,1,0:T(4,128)}, u32[]{:S(2)}) copy-start(f32[2,4,24]{2,1,0:T(4,128)} %decay_total.1) | copy-start | bytes 2308
  3.5 18.6 %copy-start = (bf16[1536,512]{1,0:T(8,128)(2,1)S(1)}, bf16[1536,512]{1,0:T(8,128)(2,1)}, u32[]{:S(2)}) copy-start(bf16[1536,512]{1,0:T(8,128)(2,1)} %weight.1) | copy-start | bytes 4718596
  3.5 9.6 %collective-permute-start = (bf16[8,4224]{1,0:T(8,128)(2,1)S(1)}, bf16[8,4224]{1,0:T(8,128)(2,1)S(1)}, u32[]{:S(2)}, u32[]{:S(2)}) collective-permute-start(bf16[8,4224]{1,0:T(8,128)(2,1)S(1)} %get-tuple-element.35), channel_id=1, source_target_pairs={{0,4},{2,6},{4,0},{6,2},{1,5},{3,7},{5,1},{7,3},{8,12},{10,14},{12... | collective-permute-start | bytes 202760 | tf_op jit(solution)/shard_map/ppermute | solution.py:38
  7.6 6.2 %collective-permute-start.1 = (bf16[8,4224]{1,0:T(8,128)(2,1)S(1)}, bf16[8,4224]{1,0:T(8,128)(2,1)S(1)}, u32[]{:S(2)}, u32[]{:S(2)}) collective-permute-start(bf16[8,4224]{1,0:T(8,128)(2,1)S(1)} %get-tuple-element.36), channel_id=1, source_target_pairs={{0,6},{2,4},{4,2},{6,0},{1,7},{3,5},{5,3},{7,1},{8,14},{10,12},{12... | collective-permute-start | bytes 202760 | tf_op jit(solution)/shard_map/ppermute | solution.py:38
  9.0 5.0 %collective-permute-start.2 = (bf16[8,4224]{1,0:T(8,128)(2,1)S(1)}, bf16[8,4224]{1,0:T(8,128)(2,1)S(1)}, u32[]{:S(2)}, u32[]{:S(2)}) collective-permute-start(bf16[8,4224]{1,0:T(8,128)(2,1)S(1)} %get-tuple-element.37), channel_id=1, source_target_pairs={{0,2},{2,0},{4,6},{6,4},{1,3},{3,1},{5,7},{7,5},{8,10},{10,8},{12,... | collective-permute-start | bytes 202760 | tf_op jit(solution)/shard_map/ppermute | solution.py:38
  14.6 5.8 %collective-permute-start.5 = (bf16[8,1536]{1,0:T(8,128)(2,1)S(1)}, bf16[8,1536]{1,0:T(8,128)(2,1)S(1)}, u32[]{:S(2)}, u32[]{:S(2)}) collective-permute-start(bf16[8,1536]{1,0:T(8,128)(2,1)S(1)} %get-tuple-element.38.rest_0_), channel_id=1, source_target_pairs={{0,2},{2,4},{4,6},{6,0},{1,3},{3,5},{5,7},{7,1},{8,10},{10,12},{12... | collective-permute-start | bytes 73736 | tf_op jit(solution)/shard_map/ppermute | solution.py:38
  15.5 5.3 %collective-permute-start.4 = (bf16[8,1536]{1,0:T(8,128)(2,1)S(1)}, bf16[8,1536]{1,0:T(8,128)(2,1)S(1)}, u32[]{:S(2)}, u32[]{:S(2)}) collective-permute-start(bf16[8,1536]{1,0:T(8,128)(2,1)S(1)} %get-tuple-element.38.rest_0_), channel_id=1, source_target_pairs={{0,4},{2,6},{4,0},{6,2},{1,5},{3,7},{5,1},{7,3},{8,12},{10,14},{12... | collective-permute-start | bytes 73736 | tf_op jit(solution)/shard_map/ppermute | solution.py:38
  18.3 3.8 %collective-permute-start.3 = (bf16[8,1536]{1,0:T(8,128)(2,1)S(1)}, bf16[8,1536]{1,0:T(8,128)(2,1)S(1)}, u32[]{:S(2)}, u32[]{:S(2)}) collective-permute-start(bf16[8,1536]{1,0:T(8,128)(2,1)S(1)} %get-tuple-element.38.rest_0_), channel_id=1, source_target_pairs={{0,6},{2,0},{4,2},{6,4},{1,7},{3,1},{5,3},{7,5},{8,14},{10,8},{12,... | collective-permute-start | bytes 73736 | tf_op jit(solution)/shard_map/ppermute | solution.py:38
  22.5 1.2 %collective-permute-start.6 = (bf16[8,4,512]{2,1,0:T(4,128)(2,1)S(1)}, bf16[8,4,512]{2,1,0:T(4,128)(2,1)S(1)}, u32[]{:S(2)}, u32[]{:S(2)}) collective-permute-start(bf16[8,4,512]{2,1,0:T(4,128)(2,1)S(1)} %mix.1), channel_id=1, source_target_pairs={{0,1},{1,0},{2,3},{3,2},{4,5},{5,4},{6,7},{7,6},{8,9},{9,8},{10,11... | collective-permute-start | bytes 98312 | tf_op jit(solution)/shard_map/ppermute | solution.py:38

commit v5 on v4

--- a/solution.py
+++ b/solution.py
@@ -270,25 +270,32 @@
                 value = value + update[i * HEAD_DIM : (i + 1) * HEAD_DIM]
                 state[s, h] = value
                 state_low[s, h * HEAD_DIM : (h + 1) * HEAD_DIM, :] = value.astype(bf16)
-        leave(s)
+            leave(s, g * per_group, per_group)
 
 
 def fetched_state_kernel(n_tp, acc, state_hbm, *rest):
     sources, new_state, outs, rest = rest[:11], rest[11], rest[12:19], rest[19:]
-    gain_rows, state, targets, sems, state_sems = rest[0], rest[1], rest[2:13], rest[13], rest[14]
+    gain_rows, state, targets = rest[0], rest[1], rest[2:13]
+    sems, state_sems, out_sems = rest[13:]
     own = state.shape[0]
     small = [
         pltpu.make_async_copy(source, target, sems.at[i])
         for i, (source, target) in enumerate(zip(sources, targets, strict=True))
     ]
     inward = [
-        pltpu.make_async_copy(state_hbm.at[s], state.at[s], state_sems.at[0, s])
+        pltpu.make_async_copy(state_hbm.at[s], state.at[s], state_sems.at[s])
         for s in range(own)
     ]
-    outward = [
-        pltpu.make_async_copy(state.at[s], new_state.at[s], state_sems.at[1, s])
-        for s in range(own)
-    ]
+    outward = []
+
+    def leave(s, first, count):
+        part = pl.ds(first, count)
+        copy = pltpu.make_async_copy(
+            state.at[s, part], new_state.at[s, part], out_sems.at[len(outward)]
+        )
+        copy.start()
+        outward.append(copy)
+
     for copy in small + inward:
         copy.start()
     for copy in small:
@@ -296,7 +303,7 @@
     state_kernel(
         n_tp,
         lambda s: inward[s].wait(),
-        lambda s: outward[s].start(),
+        leave,
         acc,
         state,
         *targets,
@@ -579,7 +586,8 @@
             pltpu.VMEM((n_tp * width // LANES, LANES), f32),
             *(pltpu.VMEM(array.shape, array.dtype) for array in later),
             pltpu.SemaphoreType.DMA((len(later) - 1,)),
-            pltpu.SemaphoreType.DMA((2, own)),
+            pltpu.SemaphoreType.DMA((own,)),
+            pltpu.SemaphoreType.DMA((own * (bc // STATE),)),
         ],
         out_specs=[hbm] + [vmem] * 7,
         compiler_params=params(12),

time: 24.5 us -> 24.5 us (level)
  transfers between devices with their start and end apart: 7 -> 7, of which waited for: 5 -> 5; matrix products, arithmetic and copies ran while one was open for 0% -> 0% of each run, Pallas kernels for 19% -> 18%
where the time goes in v5:
time: 24.5 us; the launch traced here: 24.3 us
  starting transfers between devices  11.5 us (47%)
  Pallas kernels  8.29 us (34%)
  waiting for transfers between devices  3.23 us (13%)
  between operations  0.7 us (3%)
  other arithmetic  0.64 us (3%)
    ppermute x7, starting transfers between devices, permute(): lax.ppermute(array, axis, [(i, peer(i, k, n, ring)) for i in range(n)])  11.5 us
    pallas_call x1, Pallas kernels, local(): pl.pallas_call(functools.partial(fetched_state_kernel, n_tp), out_shape=[...  3.82 us
    ppermute x7, waiting for transfers between devices, permute(): lax.ppermute(array, axis, [(i, peer(i, k, n, ring)) for i in range(n)])  3.23 us
    pallas_call x1, Pallas kernels, local(): pl.pallas_call(functools.partial(project_kernel, n_kv, n_tp, chunk), out_...  2.82 us
    pallas_call x1, Pallas kernels, local(): pl.pallas_call(outputs_kernel, out_shape=[sds((own, props, width), bf16),...  0.67 us
    convert_element_type x1, other arithmetic, local(): total.astype(bf16)  0.64 us
    pallas_call x1, Pallas kernels, local(): pl.pallas_call(functools.partial(mixer_kernel, local_d * n_kv, len(got)),...  0.62 us
  transfers between devices with their start and end apart: 7, of which 5 were waited for; matrix products, arithmetic and copies ran while one was open for 0% of the time, Pallas kernels for 18%

profile of v5, /device:TPU:0, one launch (start us, length us, event | category | flops | bytes accessed | tf_op | source)
XLA Modules:
  0.0 24.3 jit_solution(16109155604495617768)
XLA Ops:
  0.6 0.0 copy-start.2
  0.6 2.8 %project.1 = (bf16[8,4224]{1,0:T(8,128)(2,1)S(1)}, bf16[8,4224]{1,0:T(8,128)(2,1)S(1)}, bf16[8,4224]{1,0:T(8,128)(2,1)S(1)}, bf16[8,4224]{1,0:T(8,128)(2,1)S(1)}) custom-call(bf16[8,4,512]{2,1,0:T(4,128)(2,1)} %tok_hbm.1, bf16[16,128]{1,0:T(8,128)(2,1)} %bitcast.11, bf16[512,1536]{1,0:T(8,128)(2,1)} %wx.1, bf16[512,2,512]{2,1,0:T(2,128)(2,1)} %wm.1, ...), custom_call_target="tpu_custom_call" | custom-call | tf_op jit(solution)/shard_map/project/pallas_call | solution.py:513
  3.5 0.0 copy-start.1
  3.5 0.0 copy-start
  3.5 4.1 %collective-permute-start = (bf16[8,4224]{1,0:T(8,128)(2,1)S(1)}, bf16[8,4224]{1,0:T(8,128)(2,1)S(1)}, u32[]{:S(2)}, u32[]{:S(2)}) collective-permute-start(bf16[8,4224]{1,0:T(8,128)(2,1)S(1)} %get-tuple-element.35), channel_id=1, source_target_pairs={{0,4},{2,6},{4,0},{6,2},{1,5},{3,7},{5,1},{7,3},{8,12},{10,14},{12... | collective-permute-start | bytes 202760 | tf_op jit(solution)/shard_map/ppermute | solution.py:38
  7.6 1.3 %collective-permute-start.1 = (bf16[8,4224]{1,0:T(8,128)(2,1)S(1)}, bf16[8,4224]{1,0:T(8,128)(2,1)S(1)}, u32[]{:S(2)}, u32[]{:S(2)}) collective-permute-start(bf16[8,4224]{1,0:T(8,128)(2,1)S(1)} %get-tuple-element.36), channel_id=1, source_target_pairs={{0,6},{2,4},{4,2},{6,0},{1,7},{3,5},{5,3},{7,1},{8,14},{10,12},{12... | collective-permute-start | bytes 202760 | tf_op jit(solution)/shard_map/ppermute | solution.py:38
  9.0 0.2 collective-permute-start.2
  9.2 0.0 copy-done.2
  9.2 3.8 %state.1 = (f32[2,24,64,128]{3,2,1,0:T(8,128)}, bf16[2,1536,128]{2,1,0:T(8,128)(2,1)S(1)}, bf16[3,2,1536]{2,1,0:T(2,128)(2,1)S(1)}, bf16[2,3,2,512]{3,2,1,0:T(2,...) custom-call(s32[2]{0:T(128)S(1)} %copy-done.2, ...), custom_call_target="tpu_custom_call" | custom-call | tf_op jit(solution)/shard_map/state/pallas_call | solution.py:572
  13.0 0.0 collective-permute-done.rest_1_
  13.0 0.8 %collective-permute-done.1.rest_2_ = bf16[8,4224]{1,0:T(8,128)(2,1)S(1)} collective-permute-done((bf16[8,4224]{1,0:T(8,128)(2,1)S(1)}, bf16[8,4224]{1,0:T(8,128)(2,1)S(1)}, u32[]{:S(2)}, u32[]{:S(2)}) %collective-permute-start.1) | collective-permute-done | bytes 67616 | tf_op jit(solution)/shard_map/ppermute | solution.py:38
  13.9 0.1 collective-permute-done.2.rest_3_
  14.0 0.0 copy-done.1
  14.0 0.6 %mixer.1 = (bf16[8,1536]{1,0:T(8,128)(2,1)S(1)}, bf16[8,2560]{1,0:T(8,128)(2,1)S(1)}, f32[8,1536]{1,0:T(8,128)S(1)}, f32[8,512]{1,0:T(8,128)S(1)}, f32[8,24]{1,0:T(8,128)S(1)}) custom-call(f32[2,4,24]{2,1,0:T(4,128)S(1)} %copy-done.1, bf16[2,1536,128]{2,1,0:T(8,128)(2,1)S(1)} %get-tuple-element.29.state_low, f32[8,2560]{1,0:T(8,128)S(1)} %get-tuple-element.30.conv_tail, ...), custom_call_target="tpu_custom_call" | custom-call | tf_op jit(solution)/shard_map/mixer/pallas_call | solution.py:597
  14.6 0.9 %collective-permute-start.5 = (bf16[8,1536]{1,0:T(8,128)(2,1)S(1)}, bf16[8,1536]{1,0:T(8,128)(2,1)S(1)}, u32[]{:S(2)}, u32[]{:S(2)}) collective-permute-start(bf16[8,1536]{1,0:T(8,128)(2,1)S(1)} %get-tuple-element.38.rest_0_), channel_id=1, source_target_pairs={{0,2},{2,4},{4,6},{6,0},{1,3},{3,5},{5,7},{7,1},{8,10},{10,12},{12... | collective-permute-start | bytes 73736 | tf_op jit(solution)/shard_map/ppermute | solution.py:38
  15.5 2.8 %collective-permute-start.4 = (bf16[8,1536]{1,0:T(8,128)(2,1)S(1)}, bf16[8,1536]{1,0:T(8,128)(2,1)S(1)}, u32[]{:S(2)}, u32[]{:S(2)}) collective-permute-start(bf16[8,1536]{1,0:T(8,128)(2,1)S(1)} %get-tuple-element.38.rest_0_), channel_id=1, source_target_pairs={{0,4},{2,6},{4,0},{6,2},{1,5},{3,7},{5,1},{7,3},{8,12},{10,14},{12... | collective-permute-start | bytes 73736 | tf_op jit(solution)/shard_map/ppermute | solution.py:38
  18.3 2.1 %collective-permute-start.3 = (bf16[8,1536]{1,0:T(8,128)(2,1)S(1)}, bf16[8,1536]{1,0:T(8,128)(2,1)S(1)}, u32[]{:S(2)}, u32[]{:S(2)}) collective-permute-start(bf16[8,1536]{1,0:T(8,128)(2,1)S(1)} %get-tuple-element.38.rest_0_), channel_id=1, source_target_pairs={{0,6},{2,0},{4,2},{6,4},{1,7},{3,1},{5,3},{7,5},{8,14},{10,8},{12,... | collective-permute-start | bytes 73736 | tf_op jit(solution)/shard_map/ppermute | solution.py:38
  20.4 0.0 collective-permute-done.5.rest_3_
  20.4 0.4 %collective-permute-done.4.rest_2_ = bf16[8,1536]{1,0:T(8,128)(2,1)S(1)} collective-permute-done((bf16[8,1536]{1,0:T(8,128)(2,1)S(1)}, bf16[8,1536]{1,0:T(8,128)(2,1)S(1)}, u32[]{:S(2)}, u32[]{:S(2)}) %collective-permute-start.4) | collective-permute-done | bytes 24608 | tf_op jit(solution)/shard_map/ppermute | solution.py:38
  20.8 1.3 %collective-permute-done.3.rest_1_ = bf16[8,1536]{1,0:T(8,128)(2,1)S(1)} collective-permute-done((bf16[8,1536]{1,0:T(8,128)(2,1)S(1)}, bf16[8,1536]{1,0:T(8,128)(2,1)S(1)}, u32[]{:S(2)}, u32[]{:S(2)}) %collective-permute-start.3) | collective-permute-done | bytes 24608 | tf_op jit(solution)/shard_map/ppermute | solution.py:38
  22.1 0.0 copy-done
  22.1 0.4 %mix.1 = bf16[8,4,512]{2,1,0:T(4,128)(2,1)S(1)} custom-call(bf16[1536,512]{1,0:T(8,128)(2,1)S(1)} %copy-done, bf16[8,1536]{1,0:T(8,128)(2,1)S(1)} %get-tuple-element.38.rest_0_, bf16[8,1536]{1,0:T(8,128)(2,1)S(1)} %collective-permute-done.3.rest_1_, bf16[8,1536]{1,0:T(8,128)(2,1)S(1)} %collective-permute-done.4.rest_2_, ...), custom_call_target="tpu_custom_call" | custom-call | tf_op jit(solution)/shard_map/mix/pallas_call | solution.py:630
  22.5 0.0 collective-permute-start.6
  22.5 0.7 %outputs.1 = (bf16[2,4,1536]{2,1,0:T(4,128)(2,1)}, bf16[2,4,512]{2,1,0:T(4,128)(2,1)}, f32[2,4,24]{2,1,0:T(4,128)}, bf16[7,2,1536]{2,1,0:T(2,128)(2,1)}, bf16[2,7,2,512]{3,2,1,0:T(2,128)(2,1)}) custom-call(bf16[8,2560]{1,0:T(8,128)(2,1)S(1)} %get-tuple-element.40.raw, f32[8,1536]{1,0:T(8,128)S(1)} %get-tuple-element.41.weighted, ...), custom_call_target="tpu_custom_call" | custom-call | tf_op jit(solution)/shard_map/outputs/pallas_call | solution.py:617
  23.2 0.5 %collective-permute-done.6 = bf16[8,4,512]{2,1,0:T(4,128)(2,1)S(1)} collective-permute-done((bf16[8,4,512]{2,1,0:T(4,128)(2,1)S(1)}, bf16[8,4,512]{2,1,0:T(4,128)(2,1)S(1)}, u32[]{:S(2)}, u32[]{:S(2)}) %collective-permute-start.6) | collective-permute-done | bytes 32800 | tf_op jit(solution)/shard_map/ppermute | solution.py:38
  23.7 0.6 %add_convert_fusion = bf16[8,4,512]{2,1,0:T(4,128)(2,1)} fusion(bf16[8,4,512]{2,1,0:T(4,128)(2,1)S(1)} %collective-permute-done.6, bf16[8,4,512]{2,1,0:T(4,128)(2,1)S(1)} %mix.1), kind=kLoop, calls=%fused_computation | loop fusion | flops 65536 | bytes 98304 | tf_op jit(solution)/shard_map/convert_element_type | solution.py:640
Async XLA Ops:
  0.6 8.6 %copy-start.2 = (s32[2]{0:T(128)S(1)}, s32[2]{0:T(128)}, u32[]{:S(2)}) copy-start(s32[2]{0:T(128)} %acc.1) | copy-start | bytes 28
  3.5 10.5 %copy-start.1 = (f32[2,4,24]{2,1,0:T(4,128)S(1)}, f32[2,4,24]{2,1,0:T(4,128)}, u32[]{:S(2)}) copy-start(f32[2,4,24]{2,1,0:T(4,128)} %decay_total.1) | copy-start | bytes 2308
  3.5 18.6 %copy-start = (bf16[1536,512]{1,0:T(8,128)(2,1)S(1)}, bf16[1536,512]{1,0:T(8,128)(2,1)}, u32[]{:S(2)}) copy-start(bf16[1536,512]{1,0:T(8,128)(2,1)} %weight.1) | copy-start | bytes 4718596
  3.5 9.5 %collective-permute-start = (bf16[8,4224]{1,0:T(8,128)(2,1)S(1)}, bf16[8,4224]{1,0:T(8,128)(2,1)S(1)}, u32[]{:S(2)}, u32[]{:S(2)}) collective-permute-start(bf16[8,4224]{1,0:T(8,128)(2,1)S(1)} %get-tuple-element.35), channel_id=1, source_target_pairs={{0,4},{2,6},{4,0},{6,2},{1,5},{3,7},{5,1},{7,3},{8,12},{10,14},{12... | collective-permute-start | bytes 202760 | tf_op jit(solution)/shard_map/ppermute | solution.py:38
  7.6 6.2 %collective-permute-start.1 = (bf16[8,4224]{1,0:T(8,128)(2,1)S(1)}, bf16[8,4224]{1,0:T(8,128)(2,1)S(1)}, u32[]{:S(2)}, u32[]{:S(2)}) collective-permute-start(bf16[8,4224]{1,0:T(8,128)(2,1)S(1)} %get-tuple-element.36), channel_id=1, source_target_pairs={{0,6},{2,4},{4,2},{6,0},{1,7},{3,5},{5,3},{7,1},{8,14},{10,12},{12... | collective-permute-start | bytes 202760 | tf_op jit(solution)/shard_map/ppermute | solution.py:38
  9.0 5.0 %collective-permute-start.2 = (bf16[8,4224]{1,0:T(8,128)(2,1)S(1)}, bf16[8,4224]{1,0:T(8,128)(2,1)S(1)}, u32[]{:S(2)}, u32[]{:S(2)}) collective-permute-start(bf16[8,4224]{1,0:T(8,128)(2,1)S(1)} %get-tuple-element.37), channel_id=1, source_target_pairs={{0,2},{2,0},{4,6},{6,4},{1,3},{3,1},{5,7},{7,5},{8,10},{10,8},{12,... | collective-permute-start | bytes 202760 | tf_op jit(solution)/shard_map/ppermute | solution.py:38
  14.6 5.8 %collective-permute-start.5 = (bf16[8,1536]{1,0:T(8,128)(2,1)S(1)}, bf16[8,1536]{1,0:T(8,128)(2,1)S(1)}, u32[]{:S(2)}, u32[]{:S(2)}) collective-permute-start(bf16[8,1536]{1,0:T(8,128)(2,1)S(1)} %get-tuple-element.38.rest_0_), channel_id=1, source_target_pairs={{0,2},{2,4},{4,6},{6,0},{1,3},{3,5},{5,7},{7,1},{8,10},{10,12},{12... | collective-permute-start | bytes 73736 | tf_op jit(solution)/shard_map/ppermute | solution.py:38
  15.5 5.3 %collective-permute-start.4 = (bf16[8,1536]{1,0:T(8,128)(2,1)S(1)}, bf16[8,1536]{1,0:T(8,128)(2,1)S(1)}, u32[]{:S(2)}, u32[]{:S(2)}) collective-permute-start(bf16[8,1536]{1,0:T(8,128)(2,1)S(1)} %get-tuple-element.38.rest_0_), channel_id=1, source_target_pairs={{0,4},{2,6},{4,0},{6,2},{1,5},{3,7},{5,1},{7,3},{8,12},{10,14},{12... | collective-permute-start | bytes 73736 | tf_op jit(solution)/shard_map/ppermute | solution.py:38
  18.3 3.8 %collective-permute-start.3 = (bf16[8,1536]{1,0:T(8,128)(2,1)S(1)}, bf16[8,1536]{1,0:T(8,128)(2,1)S(1)}, u32[]{:S(2)}, u32[]{:S(2)}) collective-permute-start(bf16[8,1536]{1,0:T(8,128)(2,1)S(1)} %get-tuple-element.38.rest_0_), channel_id=1, source_target_pairs={{0,6},{2,0},{4,2},{6,4},{1,7},{3,1},{5,3},{7,5},{8,14},{10,8},{12,... | collective-permute-start | bytes 73736 | tf_op jit(solution)/shard_map/ppermute | solution.py:38
  22.5 1.2 %collective-permute-start.6 = (bf16[8,4,512]{2,1,0:T(4,128)(2,1)S(1)}, bf16[8,4,512]{2,1,0:T(4,128)(2,1)S(1)}, u32[]{:S(2)}, u32[]{:S(2)}) collective-permute-start(bf16[8,4,512]{2,1,0:T(4,128)(2,1)S(1)} %mix.1), channel_id=1, source_target_pairs={{0,1},{1,0},{2,3},{3,2},{4,5},{5,4},{6,7},{7,6},{8,9},{9,8},{10,11... | collective-permute-start | bytes 98312 | tf_op jit(solution)/shard_map/ppermute | solution.py:38
